TPU v7x, 256 devices: a whole 4x4x8 slice. The times are simulated.
256 devices in a mesh: sp: 32 (over z, y), tp: 8 (over x, core).
Axes of the slice: x: 4, y: 4, z: 8, core: 2. Of those that a mesh axis runs over, the one named last changes fastest.
Arguments:
- queries: bfloat16 [9216, 2048], P('sp', 'tp'), as said below
- key_vectors: bfloat16 [9216, 2048], P('sp', 'tp'), as said below
- latents: bfloat16 [9216, 2048], P('sp'), as said below
- value_weight: bfloat16 [2048, 2048], P(None, 'tp'), as said below
- log_sums: float32 [9216, 32], P('sp', 'tp'), as said below
- out_first: bfloat16 [9216, 2048], P('sp', 'tp'), as said below
- out_second: bfloat16 [9216, 2048], P('sp', 'tp'), as said below
- cotangent: bfloat16 [9216, 2048], P('sp', 'tp'), may hold values from -6 to 6
- head_lambda: float32 [16], P('tp'), may hold values from 0.3 to 0.8
Outputs:
- grad_queries: float32 [9216, 2048], P('sp', 'tp')
- grad_keys: float32 [9216, 2048], P('sp', 'tp')
- grad_latents: bfloat16 [9216, 2048], P('sp', 'tp')
- grad_weight: float32 [2048, 2048], P('sp', 'tp')
Inputs may be any that keep to these rules, and one draw needn't show every extreme that they name: queries with entries of standard deviation 1.75. `key_vectors`: keys with entries of standard deviation 1. `latents`: inputs of standard deviation 1. `value_weight`: weights scaled by the inverse square root of 2048. `log_sums`: each row's log-sum of exponentials of its causal scores, for the given queries and keys. `out_first`: the first map's attention output for the given queries, keys, values and log-sums. `out_second`: the second map's attention output, likewise.
All inputs are finite; a program needn't handle non-finite values.
Results may differ from a plain program's by a relative error of at most 0.022.
Values may be sent and summed in bfloat16 or wider, within the bound.
No kernel may reach another device: no remote copies, remote signals or barrier semaphores. Data moves between devices by JAX's collectives and lax.ppermute only.
A program may use at most 192 MiB of HBM per device.

v0:
```python
import jax
import jax.numpy as jnp
from jax import lax
from jax.sharding import PartitionSpec as P

DH = 64
DV = 128


def side_by_side(arrays, axis, dim, along):
    widths = [a.shape[along] for a in arrays]
    both = jnp.concatenate(arrays, axis=along)
    out = lax.all_gather(both, axis, axis=dim, tiled=True)
    return tuple(jnp.split(out, [sum(widths[:k]) for k in range(1, len(widths))], axis=along))


def cut_along(x, dim, devices):
    before, after = (x.shape[:dim], x.shape[dim + 1 :])
    return jnp.moveaxis(x.reshape(*before, devices, -1, *after), dim, 0)


def summed_on_arrival(x, axis, dim):
    parts = cut_along(x, dim, lax.axis_size(axis))
    arrived = lax.all_to_all(parts, axis, split_axis=0, concat_axis=0, tiled=True)
    return arrived.astype(jnp.float32).sum(axis=0)


def row_terms(out_first, out_second, cotangent, head_lambda):
    count = out_first.shape[0]
    head_count = head_lambda.shape[0]
    first = out_first.astype(jnp.float32).reshape(count, head_count, DV)
    second = out_second.astype(jnp.float32).reshape(count, head_count, DV)
    mixed = first - head_lambda[None, :, None] * second
    inverse = lax.rsqrt(jnp.mean(mixed * mixed, axis=-1, keepdims=True) + 1e-06)
    normed = mixed * inverse
    grad_out = cotangent.astype(jnp.float32).reshape(count, head_count, DV)
    grad_mixed = inverse * (grad_out - normed * jnp.mean(grad_out * normed, axis=-1, keepdims=True))
    grad_rows = grad_mixed.astype(jnp.bfloat16)
    widened = lax.optimization_barrier(grad_rows).astype(jnp.float32)
    row_dots = jnp.stack(
        [jnp.sum(widened * first, axis=-1), jnp.sum(widened * second, axis=-1)], axis=-1
    )
    return (grad_rows.reshape(count, head_count * DV), row_dots.reshape(count, head_count * 2))


def block_grads(
    query_rows, grad_rows, lse_rows, dot_rows, query_pos, key_rows, value_rows, key_pos, head_lambda
):
    count = query_rows.shape[0]
    width = key_rows.shape[0]
    head_count = head_lambda.shape[0]
    score_scale = DH ** (-0.5)
    query_heads = query_rows.reshape(count, head_count, 2, DH)
    key_heads = key_rows.reshape(width, head_count, 2, DH)
    grad_heads = grad_rows.reshape(count, head_count, DV)
    value_heads = value_rows.reshape(width, head_count, DV)
    scores = (
        jnp.einsum("nhad,mhad->hanm", query_heads, key_heads, preferred_element_type=jnp.float32)
        * score_scale
    )
    causal = query_pos[:, None] >= key_pos[None, :]
    shifts = lse_rows.reshape(count, head_count, 2).transpose(1, 2, 0)[..., None]
    probs = jnp.exp(jnp.where(causal, scores - shifts, -1e30))
    d_attn = jnp.einsum("nhe,mhe->hnm", grad_heads, value_heads, preferred_element_type=jnp.float32)
    dots = dot_rows.reshape(count, head_count, 2).transpose(1, 2, 0)[..., None]
    map_weight = jnp.stack([jnp.ones_like(head_lambda), -head_lambda], axis=1)[:, :, None, None]
    d_scores = (map_weight * probs * (d_attn[:, None] - dots)).astype(jnp.bfloat16)
    weights = (probs[:, 0] - head_lambda[:, None, None] * probs[:, 1]).astype(jnp.bfloat16)
    grad_q = (
        jnp.einsum("hanm,mhad->nhad", d_scores, key_heads, preferred_element_type=jnp.float32)
        * score_scale
    )
    grad_k = (
        jnp.einsum("hanm,nhad->mhad", d_scores, query_heads, preferred_element_type=jnp.float32)
        * score_scale
    )
    grad_v = jnp.einsum("hnm,nhe->mhe", weights, grad_heads, preferred_element_type=jnp.float32)
    return (grad_q.reshape(count, -1), grad_k.reshape(width, -1), grad_v.reshape(width, -1))


def per_device(
    queries,
    key_vectors,
    latents,
    value_weight,
    log_sums,
    out_first,
    out_second,
    cotangent,
    head_lambda,
):
    local_rows = queries.shape[0]
    offset = lax.axis_index("sp") * local_rows
    positions = offset + jnp.arange(local_rows, dtype=jnp.int32)
    last_row = offset + local_rows - 1
    values = jnp.dot(latents, value_weight, preferred_element_type=jnp.float32).astype(jnp.bfloat16)
    grad_rows, row_dots = row_terms(out_first, out_second, cotangent, head_lambda)
    gathered_stats = side_by_side((log_sums, row_dots), "sp", 0, 1)
    key_rows, value_rows = side_by_side((key_vectors, values), "sp", 0, 1)
    count = key_rows.shape[0]

    def compute(current):
        key_pos = jnp.arange(count, dtype=jnp.int32)
        grad_q, unused_k, unused_v = block_grads(
            queries,
            grad_rows,
            log_sums,
            row_dots,
            positions,
            key_rows,
            value_rows,
            key_pos,
            head_lambda,
        )
        return grad_q

    grad_queries = lax.cond(
        jnp.int32(0) <= last_row,
        compute,
        lambda current: current,
        jnp.zeros((local_rows, queries.shape[1]), jnp.float32),
    )
    start_totals = (
        jnp.zeros((local_rows, key_vectors.shape[1]), jnp.float32),
        jnp.zeros((local_rows, values.shape[1]), jnp.float32),
    )
    query_rows, grad_piece = side_by_side((queries, grad_rows), "sp", 0, 1)
    add_count = query_rows.shape[0]

    def compute(current):
        query_pos = jnp.arange(add_count, dtype=jnp.int32)
        lse_rows = gathered_stats[0]
        dot_rows = gathered_stats[1]
        unused_q, grad_k, grad_v = block_grads(
            query_rows,
            grad_piece,
            lse_rows,
            dot_rows,
            query_pos,
            key_vectors,
            values,
            positions,
            head_lambda,
        )
        return (grad_k, grad_v)

    grad_keys, grad_values = lax.cond(
        jnp.int32(0) + add_count - 1 >= offset, compute, lambda current: current, start_totals
    )
    values_grad = grad_values.astype(jnp.bfloat16)
    grad_weight = summed_on_arrival(
        lax.dot_general(
            latents, values_grad, (((0,), (0,)), ((), ())), preferred_element_type=jnp.float32
        ).astype(jnp.bfloat16),
        "sp",
        0,
    )
    latent_partial = lax.dot_general(
        values_grad, value_weight, (((1,), (1,)), ((), ())), preferred_element_type=jnp.float32
    )
    grad_latents = lax.psum_scatter(
        latent_partial.astype(jnp.bfloat16), "tp", scatter_dimension=1, tiled=True
    )
    return (grad_queries, grad_keys, grad_latents, grad_weight)


def solution(mesh):
    return jax.shard_map(
        per_device,
        mesh=mesh,
        in_specs=(
            P("sp", "tp"),
            P("sp", "tp"),
            P("sp", None),
            P(None, "tp"),
            P("sp", "tp"),
            P("sp", "tp"),
            P("sp", "tp"),
            P("sp", "tp"),
            P("tp"),
        ),
        out_specs=(P("sp", "tp"), P("sp", "tp"), P("sp", "tp"), P("sp", "tp")),
        check_vma=False,
    )
```

profile of v0, /device:TPU:8, one launch (start us, length us, event | category | flops | bytes accessed | tf_op | source)
XLA Modules:
  0.0 307.0 jit_solution(7757270281936150602)
XLA Ops:
  13.4 1.6 pad_maximum_fusion.1
  15.2 1.7 convolution_convert_fusion.2
  16.9 1.6 pad_maximum_fusion
  20.6 52.6 %all-gather = f32[32,288,8]{1,2,0:T(8,128)S(1)} all-gather(f32[1,288,8]{1,2,0:T(8,128)S(1)} %maximum_bitcast_fusion), channel_id=1, replica_groups=mesh['sp'=32,'tp'=8] {'sp'}, dimensions={0}, use_global_device_ids=true | all-gather | bytes 304128 | tf_op jit(solution)/shard_map/all_gather | solution.py:13
  73.5 46.7 %all-gather.6.cloned.1.call-done = bf16[9216,512]{1,0:T(8,128)(2,1)} async-done(((bf16[288,512]{1,0:T(8,128)(2,1)}), bf16[9216,512]{1,0:T(8,128)(2,1)}) %all-gather.6.cloned.1.call-update) | async-done | bytes 9437200 | tf_op jit(solution)/shard_map/all_gather | solution.py:13
  120.2 97.8 %conditional.3 = (bf16[288,256]{1,0:T(8,128)(2,1)S(1)}, f32[288,256]{1,0:T(8,128)S(1)}) conditional(s32[]{:T(128)} %convert_element_type.67, () %tuple.26, (f32[2]{0:T(128)S(1)}, s32[288]{0:T(512)S(1)}, bf16[9216,512]{1,0:T(8,128)(2,1)}, bf16[288,256]{1,0:T(8,128)(2,1)S(1)}, f32[9216,8]{0,1:T(8,128)S(1)}, ...), branch_computations={%region_6.7_spmd, %region_7.8_spmd} | conditional | flops 5528862720 | bytes 235193568 | solution.py:147
  120.2 12.9 %copy.135 = bf16[9216,512]{0,1:T(8,128)(2,1)} copy(bf16[9216,512]{1,0:T(8,128)(2,1)} %get-tuple-element.144) | data formatting | bytes 18874368 | tf_op jit(solution)/shard_map
  133.1 8.2 %fusion.35 = (bf16[9216,256]{0,1:T(8,128)(2,1)}, bf16[9216,256]{0,1:T(8,128)(2,1)}) fusion(bf16[9216,512]{0,1:T(8,128)(2,1)} %copy.135), kind=kLoop, calls=%fused_computation.62 | loop fusion | bytes 18874368 | tf_op jit(solution)/shard_map/split | solution.py:14
  141.5 2.9 iota_compare_fusion.1
  144.6 21.1 %select_exponential_fusion = f32[2,2,9216,288]{2,3,1,0:T(8,128)} fusion(f32[2,2,9216]{2,1,0:T(2,128)S(1)} %bitcast.141, pred[9216,288]{0,1:T(8,128)(4,1)} %iota_compare_fusion.1, bf16[9216,2,2,64]{0,3,2,1:T(8,128)(2,1)} %bitcast.128, bf16[288,2,2,64]{0,3,2,1:T(8,128)(2,1)S(1)} %bitcast.140), kind=kOutput, calls=%fused_computation.10 | convolution fusion | flops 1390804992 | bytes 50135040 | tf_op jit(solution)/shard_map/cond/branch_1_fun/nhad,mhad->hanm/dot_general | solution.py:58
  165.6 16.9 %fusion.17 = bf16[2,36,8,128]{3,2,1,0:T(8,128)(2,1)S(1)} fusion(bf16[9216,2,128]{0,2,1:T(8,128)(2,1)} %bitcast.126, f32[2,2,9216,288]{2,3,1,0:T(8,128)} %select_exponential_fusion, f32[2]{0:T(128)S(1)} %get-tuple-element.46), kind=kOutput, calls=%fused_computation.21 | convolution fusion | flops 1374953472 | bytes 47333384 | tf_op jit(solution)/shard_map/cond/branch_1_fun/hnm,nhe->mhe/dot_general | solution.py:77
  182.7 11.2 %fusion.20 = f32[2,9216,288]{1,2,0:T(8,128)} fusion(bf16[9216,2,128]{0,2,1:T(8,128)(2,1)} %bitcast.127, bf16[288,256]{1,0:T(8,128)(2,1)S(1)} %get-tuple-element.51), kind=kOutput, calls=%fused_computation.23 | convolution fusion | flops 1358954496 | bytes 26099712 | tf_op jit(solution)/shard_map/cond/branch_1_fun/nhe,mhe->hnm/dot_general | solution.py:64
  194.1 23.8 %fusion.13 = f32[2,2,288,64]{2,3,1,0:T(8,128)S(1)} fusion(bf16[9216,2,2,64]{0,3,2,1:T(8,128)(2,1)} %bitcast.129, f32[2,2,9216,288]{2,3,1,0:T(8,128)} %select_exponential_fusion, f32[2,2,9216]{2,1,0:T(2,128)S(1)} %bitcast.132, f32[2,9216,288]{1,2,0:T(8,128)} %fusion.20, f32[2,2]{1,0:T(2,128)S(1)} %stack.17.clone), kind=kOutput, calls=%fused_computation.19 | convolution fusion | flops 1401495552 | bytes 68861968 | tf_op jit(solution)/shard_map/cond/branch_1_fun/hanm,nhad->mhad/dot_general | solution.py:74
  218.1 2.9 convolution_convert_fusion
  221.7 1.3 copy.137
  223.0 7.3 %all-to-all-start = ((bf16[32,64,256]{2,1,0:T(8,128)(2,1)}), bf16[32,64,256]{2,1,0:T(8,128)(2,1)S(1)}, u32[]{:S(2)}, u32[]{:S(2)}) async-start(bf16[32,64,256]{2,1,0:T(8,128)(2,1)} %bitcast.24), calls=%async_computation.1 | async-start | bytes 2097152 | tf_op jit(solution)/shard_map/all_to_all | solution.py:24
  230.4 68.7 %conditional.2 = (f32[288,256]{1,0:T(8,128)S(1)}) conditional(s32[]{:T(128)} %convert_element_type.60, () %tuple.24, (f32[2]{0:T(128)S(1)}, s32[288]{0:T(512)S(1)}, bf16[288,256]{1,0:T(8,128)(2,1)S(1)}, bf16[9216,512]{1,0:T(8,128)(2,1)}, f32[288,4]{0,1:T(4,128)S(1)}, /*index=5*/bf16[9216,512]{1,0:T(8,128)(2,1)}, bf16[288,2,128]{2,0,1:T(8,128)(2,1)S(1)}, ...), branch_computations={%region_4.0_spmd, %region_5.6_spmd} | conditional | flops 4153909248 | bytes 120048872 | solution.py:117
  230.4 12.7 %copy.130 = bf16[9216,512]{0,1:T(8,128)(2,1)} copy(bf16[9216,512]{1,0:T(8,128)(2,1)} %get-tuple-element.139) | data formatting | bytes 18874368 | tf_op jit(solution)/shard_map
  243.1 4.8 %split.26 = bf16[9216,256]{0,1:T(8,128)(2,1)} slice(bf16[9216,512]{0,1:T(8,128)(2,1)} %copy.130), slice={[0:9216], [0:256]} | slice | bytes 9437184 | tf_op jit(solution)/shard_map/split | solution.py:14
  247.9 12.7 %copy.131 = bf16[9216,512]{0,1:T(8,128)(2,1)} copy(bf16[9216,512]{1,0:T(8,128)(2,1)} %get-tuple-element.139) | data formatting | bytes 18874368 | tf_op jit(solution)/shard_map
  260.6 2.3 slice-done
  263.0 8.6 %fusion.37 = f32[2,288,9216]{2,1,0:T(8,128)} fusion(bf16[288,2,128]{2,0,1:T(8,128)(2,1)S(1)} %get-tuple-element.43, bf16[9216,2,128]{0,2,1:T(8,128)(2,1)S(1)} %bitcast.125), kind=kOutput, calls=%fused_computation.64 | convolution fusion | flops 1358954496 | bytes 26099712 | tf_op jit(solution)/shard_map/cond/branch_1_fun/nhe,mhe->hnm/dot_general | solution.py:64
  271.8 2.9 iota_compare_fusion
  274.9 24.0 %fusion.4 = f32[2,2,288,64]{2,3,1,0:T(8,128)S(1)} fusion(bf16[9216,2,2,64]{0,3,2,1:T(8,128)(2,1)} %bitcast.130, f32[2,2,288]{2,1,0:T(2,128)S(1)} %bitcast.142, f32[2,288,9216]{2,1,0:T(8,128)} %fusion.37, f32[2,2,288]{2,1,0:T(2,128)S(1)} %bitcast.143, f32[2,2]{1,0:T(2,128)S(1)} %stack.15.clone, pred[288,9216]{1,0:T(8,128)(4,1)} %iota_compare_fusion, ...), kind=kOutput, calls=%fused_computation.5 | convolution fusion | flops 2792300544 | bytes 29058064 | tf_op jit(solution)/shard_map/cond/branch_1_fun/hanm,mhad->nhad/dot_general | solution.py:70
  (66 shorter events, 12.0 us)
Async XLA Ops:
  7.2 8.0 %copy-start = (bf16[288,2048]{1,0:T(8,128)(2,1)S(1)}, bf16[288,2048]{1,0:T(8,128)(2,1)}, u32[]{:S(2)}) copy-start(bf16[288,2048]{1,0:T(8,128)(2,1)} %param.15) | copy-start | bytes 3538948
  7.2 113.0 %copy-start.7 = (f32[2]{0:T(128)S(1)}, f32[2]{0:T(128)}, u32[]{:S(2)}) copy-start(f32[2]{0:T(128)} %param.21) | copy-start | bytes 28
  7.2 113.0 %copy-start.2 = (bf16[288,256]{1,0:T(8,128)(2,1)S(1)}, bf16[288,256]{1,0:T(8,128)(2,1)}, u32[]{:S(2)}) copy-start(bf16[288,256]{1,0:T(8,128)(2,1)} %param.14) | copy-start | bytes 442372
  7.2 13.4 %copy-start.6 = (f32[288,4]{0,1:T(4,128)S(1)}, f32[288,4]{0,1:T(4,128)}, u32[]{:S(2)}) copy-start(f32[288,4]{0,1:T(4,128)} %param.17) | copy-start | bytes 13828
  7.2 113.0 %all-gather.6.cloned.1.call-start = ((), (), s32[]{:S(2)}) async-start(), calls=%async_computation.3 | async-start | bytes 9732096 | tf_op jit(solution)/shard_map/all_gather | solution.py:13
  15.1 215.2 %all-gather.4.cloned.1.call-start = ((), (), s32[]{:S(2)}) async-start(), calls=%async_computation.2 | async-start | bytes 9732096 | tf_op jit(solution)/shard_map/all_gather | solution.py:13
  18.5 281.4 %reduce-scatter.2.cloned.1.call-start = ((), (), s32[]{:S(2)}) async-start(), calls=%async_computation.4 | async-start | bytes 1327104 | tf_op jit(solution)/shard_map/reduce_scatter | solution.py:161
  120.2 110.1 %copy-start.3 = (bf16[288,256]{1,0:T(8,128)(2,1)S(1)}, bf16[288,256]{1,0:T(8,128)(2,1)}, u32[]{:S(2)}) copy-start(bf16[288,256]{1,0:T(8,128)(2,1)} %param.13) | copy-start | bytes 442372
  218.1 12.3 %copy-start.4 = (f32[288,256]{1,0:T(8,128)}, f32[288,256]{1,0:T(8,128)S(1)}, u32[]{:S(2)}) copy-start(f32[288,256]{1,0:T(8,128)S(1)} %get-tuple-element.153) | copy-start | bytes 884740
  223.0 76.1 %all-to-all-start = ((bf16[32,64,256]{2,1,0:T(8,128)(2,1)}), bf16[32,64,256]{2,1,0:T(8,128)(2,1)S(1)}, u32[]{:S(2)}, u32[]{:S(2)}) async-start(bf16[32,64,256]{2,1,0:T(8,128)(2,1)} %bitcast.24), calls=%async_computation.1 | async-start | bytes 2097152 | tf_op jit(solution)/shard_map/all_to_all | solution.py:24
  260.6 2.3 slice-start
  299.1 0.8 copy-start.5
  299.1 1.4 copy-start.1
Sparse Core Ops, SparseCore 0:
  15.2 104.9 all-gather.5
  123.4 100.2 all-gather.3
  226.8 33.7 reduce-scatter.1
where the time goes:
time: 308 us; the launch traced here: 307 us
  matrix products  111 us (36%)
  local copies, waits for them, and re-layouts  59.5 us (19%)
  blocking collectives  52.6 us (17%)
  waiting for transfers between devices  46.8 us (15%)
  other arithmetic  15.7 us (5%)
  between operations  14 us (5%)
  starting transfers between devices  7.41 us (2%)
    all_gather x1, blocking collectives, side_by_side(): out = lax.all_gather(both, axis, axis=dim, tiled=True)  52.6 us
    all_gather x2, waiting for transfers between devices, side_by_side(): out = lax.all_gather(both, axis, axis=dim, tiled=True)  46.8 us
    another operation x5, local copies, waits for them, and re-layouts  38.6 us
    dot_general x1, matrix products, block_grads(): jnp.einsum('hanm,mhad->nhad', d_scores, key_heads, preferred_element_type...  24 us
    dot_general x1, matrix products, block_grads(): jnp.einsum('hanm,nhad->mhad', d_scores, query_heads, preferred_element_ty...  23.8 us
    dot_general x1, matrix products, block_grads(): jnp.einsum('nhad,mhad->hanm', query_heads, key_heads, preferred_element_t...  21.1 us
    dot_general x2, matrix products, block_grads(): jnp.einsum('nhe,mhe->hnm', grad_heads, value_heads, preferred_element_typ...  19.9 us
    dot_general x1, matrix products, block_grads(): jnp.einsum('hnm,nhe->mhe', weights, grad_heads, preferred_element_type=jn...  16.9 us
  transfers between devices with their start and end apart: 4, of which 1 were waited for; matrix products, arithmetic and copies ran while one was open for 57% of the time, Pallas kernels for 0%

commit v1 on v0

v1 whole, which is shorter than its diff:
```python
import functools

import jax
import jax.numpy as jnp
from jax import lax
from jax.experimental import pallas as pl
from jax.experimental.pallas import tpu as pltpu
from jax.sharding import PartitionSpec as P


DH = 64
DV = 128
NZ = 8
NY = 4
STAT_ROWS = 16
GROUPS = [(0,), (1, 7), (2, 6), (3, 5), (4,)]
VMEM_LIMIT = 24 * 2**20
F32 = jnp.float32
BF16 = jnp.bfloat16
NN = (((1,), (0,)), ((), ()))
NT = (((1,), (1,)), ((), ()))
TN = (((0,), (0,)), ((), ()))


def dot(a, b, dims=NN):
    return lax.dot_general(a, b, dims, preferred_element_type=F32)


def pack_rows_kernel(lam_ref, q_ref, first_ref, second_ref, cot_ref, lse_ref, out_ref):
    n = q_ref.shape[0]
    out_ref[0:n, 0 : 2 * DV] = q_ref[...]
    piece_row = lax.broadcasted_iota(jnp.int32, (STAT_ROWS, DV), 0)
    stats = lse_ref[...]
    for h in range(2):
        cols = slice(h * DV, (h + 1) * DV)
        lam = lam_ref[h]
        first = first_ref[:, cols].astype(F32)
        second = second_ref[:, cols].astype(F32)
        mixed = first - lam * second
        inverse = lax.rsqrt(jnp.mean(mixed * mixed, axis=-1, keepdims=True) + 1e-06)
        normed = mixed * inverse
        grad_out = cot_ref[:, cols].astype(F32)
        grad_mixed = inverse * (grad_out - normed * jnp.mean(grad_out * normed, axis=-1, keepdims=True))
        grad_rows = grad_mixed.astype(BF16)
        out_ref[0:n, 2 * DV + h * DV : 2 * DV + (h + 1) * DV] = grad_rows
        widened = grad_rows.astype(F32)
        for m, side in enumerate((first, second)):
            product = widened * side
            high = product.astype(BF16)
            low = (product - high.astype(F32)).astype(BF16)
            row = 8 + 2 * h + m
            pick = jnp.where((piece_row == row) | (piece_row == row + 4), 1.0, 0.0).astype(BF16)
            stats = stats + dot(pick, high, NT) + dot(pick, low, NT)
    high = stats.astype(BF16).astype(F32)
    is_low = (lax.broadcasted_iota(jnp.int32, stats.shape, 0) & 4) != 0
    out_ref[n : n + STAT_ROWS, :] = jnp.zeros((STAT_ROWS, 4 * DV), BF16)
    out_ref[n : n + STAT_ROWS, 0:n] = jnp.where(is_low, stats - high, high).astype(BF16)


def pack_keys_kernel(key_ref, latent_ref, weight_ref, out_ref):
    out_ref[:, 0 : 2 * DV] = key_ref[...]
    out_ref[:, 2 * DV :] = dot(latent_ref[...], weight_ref[...]).astype(BF16)


def attention_kernel(offsets, first_call, last_call, zy_ref, lam_ref, *refs):
    count = len(offsets)
    row_refs, refs = refs[:count], refs[count:]
    kv_ref, refs = refs[0], refs[1:]
    if not first_call:
        acc_in, refs = refs[0], refs[1:]
    dq_refs, refs = refs[:count], refs[count:]
    if last_call:
        total_refs, (acc_ref, kz_ref) = refs[: 2 * NY], refs[2 * NY :]
    else:
        acc_ref, kz_ref = refs
    width = kv_ref.shape[0]
    n = width // NY
    z = zy_ref[0]
    y = zy_ref[1]
    tile = 384 if width % 384 == 0 else 128

    low_lanes = lax.broadcasted_iota(jnp.int32, (1, DV), 1) < DH
    for h in range(2):
        k = kv_ref[:, h * DV : (h + 1) * DV]
        kz_ref[2 * h] = jnp.where(low_lanes, k, jnp.zeros_like(k))
        kz_ref[2 * h + 1] = jnp.where(low_lanes, jnp.zeros_like(k), k)
    if first_call:
        acc_ref[...] = jnp.zeros_like(acc_ref)
    else:
        acc_ref[...] = acc_in[...]

    def cell(rows_ref, dq_ref, diagonal):
        def head(h, carry):
            cols = pl.ds(pl.multiple_of(h * DV, DV), DV)
            grad_cols = pl.ds(pl.multiple_of((h + 2) * DV, DV), DV)
            lam = lam_ref[h]
            q = rows_ref[0:n, cols] * jnp.asarray(DH ** (-0.5), BF16)
            zeros = jnp.zeros_like(q)
            q0 = jnp.where(low_lanes, q, zeros)
            q1 = jnp.where(low_lanes, zeros, q)
            g = rows_ref[0:n, grad_cols]
            stats = rows_ref[n : n + STAT_ROWS, 0:n]
            piece_row = lax.broadcasted_iota(jnp.int32, (STAT_ROWS, DV), 0)

            def stat(row):
                pick = jnp.where((piece_row == row) | (piece_row == row + 4), 1.0, 0.0)
                return jnp.concatenate([dot(stats, pick.astype(BF16), TN)] * (tile // DV), axis=1)

            lse0, lse1 = stat(2 * h), stat(2 * h + 1)
            dot0, dot1 = stat(2 * h + 8), stat(2 * h + 9)
            dq = jnp.zeros((n, DV), F32)
            both_q = jnp.concatenate([q0, q1], axis=0)
            for t in range(width // tile):
                span = slice(t * tile, (t + 1) * tile)
                k = kv_ref[span, cols]
                v = kv_ref[span, grad_cols]
                s0 = dot(q0, k, NT) - lse0
                s1 = dot(q1, k, NT) - lse1
                if diagonal:
                    key = lax.broadcasted_iota(jnp.int32, (1, tile), 1) + t * tile
                    block = (key >= n).astype(jnp.int32) + (key >= 2 * n).astype(jnp.int32) + (key >= 3 * n).astype(jnp.int32)
                    bound = jnp.where(block == 0, key, jnp.where(y + block >= NY, -1, n))
                    seen = lax.broadcasted_iota(jnp.int32, (n, tile), 0) >= bound
                    s0 = jnp.where(seen, s0, -1e30)
                    s1 = jnp.where(seen, s1, -1e30)
                p0 = jnp.exp(s0)
                p1 = lam * jnp.exp(s1)
                d_attn = dot(g, v, NT)
                ds0 = (p0 * (d_attn - dot0)).astype(BF16)
                ds1 = (p1 * (dot1 - d_attn)).astype(BF16)
                weights = (p0 - p1).astype(BF16)
                dq = dq + dot(ds0, kz_ref[2 * h, span, :]) + dot(ds1, kz_ref[2 * h + 1, span, :])
                both_ds = jnp.concatenate([ds0, ds1], axis=0)
                acc_ref[cols, span] += dot(both_q, both_ds, TN)
                acc_ref[grad_cols, span] += dot(g, weights, TN)
            dq_ref[:, cols] = dq.astype(dq_ref.dtype)
            return carry

        lax.fori_loop(0, 2, head, 0)

    for rows_ref, dq_ref, offset in zip(row_refs, dq_refs, offsets):
        if offset == 0:
            cell(rows_ref, dq_ref, True)
        else:
            pl.when(z + offset < NZ)(functools.partial(cell, rows_ref, dq_ref, False))
    if last_call:
        for t in range(width // DV):
            turned = acc_ref[:, t * DV : (t + 1) * DV].T.astype(BF16)
            start = t * DV
            while start < (t + 1) * DV:
                e = start // n
                stop = min((t + 1) * DV, (e + 1) * n)
                part = turned[start - t * DV : stop - t * DV]
                total_refs[e][start - e * n : stop - e * n, :] = part[:, 2 * DV :]
                total_refs[NY + e][start - e * n : stop - e * n, :] = part[:, : 2 * DV]
                start = stop


def weight_term_kernel(latent_ref, *refs):
    *part_refs, grad_ref, out_ref = refs
    total = part_refs[0][...].astype(F32)
    for part in part_refs[1:]:
        total = total + part[...].astype(F32)
    grads = total.astype(BF16)
    grad_ref[...] = grads
    out_ref[...] = dot(latent_ref[...], grads, TN).astype(BF16)


def latent_term_kernel(side_ref, grad_ref, weight_ref, kept_ref, sent_ref):
    grads = grad_ref[...]
    count, _, columns = kept_ref.shape
    for out_ref, side in ((kept_ref, side_ref[1]), (sent_ref, 1 - side_ref[1])):
        for j in range(count):
            rows = pl.ds(pl.multiple_of((2 * j + side) * columns, columns), columns)
            out_ref[j] = dot(grads, weight_ref[rows, :], NT).astype(BF16)


def latent_pair_kernel(side_ref, kept_ref, arrived_ref, *out_refs):
    count = kept_ref.shape[0]
    for d, out_ref in enumerate(out_refs):
        j = lax.rem(side_ref[0] + d, count)
        out_ref[...] = (kept_ref[j].astype(F32) + arrived_ref[j].astype(F32)).astype(out_ref.dtype)


def vmem(count):
    return [pl.BlockSpec(memory_space=pltpu.VMEM)] * count


def attention(offsets, first_call, last_call, zy, head_lambda, rows, keys_values, acc):
    n = keys_values.shape[0] // NY
    width = keys_values.shape[0]
    count = len(offsets)
    operands = [zy, head_lambda, *rows, keys_values] + ([] if first_call else [acc])
    total = [jax.ShapeDtypeStruct((4 * DV, width), F32)]
    if last_call:
        total = [jax.ShapeDtypeStruct((n, 2 * DV), BF16)] * (2 * NY)
    scratch = [pltpu.VMEM((4, width, DV), BF16)]
    if last_call:
        scratch = [pltpu.VMEM((4 * DV, width), F32)] + scratch
    smem = [pl.BlockSpec(memory_space=pltpu.SMEM)] * 2
    return pl.pallas_call(
        functools.partial(attention_kernel, offsets, first_call, last_call),
        out_shape=[jax.ShapeDtypeStruct((n, 2 * DV), F32 if d == 0 else BF16) for d in offsets] + total,
        in_specs=smem + vmem(len(operands) - 2),
        out_specs=vmem(count + len(total)),
        scratch_shapes=scratch,
        cost_estimate=pl.CostEstimate(flops=count * 4 * 10**9, bytes_accessed=count * 10**6, transcendentals=0),
        compiler_params=pltpu.CompilerParams(vmem_limit_bytes=VMEM_LIMIT),
    )(*operands)


def ring(size, step):
    return [(i, (i + step) % size) for i in range(size)]


def program(
    queries, key_vectors, latents, value_weight, log_sums, out_first, out_second, cotangent, head_lambda
):
    n = queries.shape[0]
    z = lax.axis_index("z")
    y = lax.axis_index("y")
    zy = jnp.stack([z, y]).astype(jnp.int32)
    sums = log_sums.T
    sums = jnp.concatenate([sums, sums, jnp.zeros((8, n), F32)], axis=0)
    rows = pl.pallas_call(
        pack_rows_kernel,
        out_shape=jax.ShapeDtypeStruct((n + STAT_ROWS, 4 * DV), BF16),
        in_specs=[pl.BlockSpec(memory_space=pltpu.SMEM)] + vmem(5),
        out_specs=vmem(1)[0],
        cost_estimate=pl.CostEstimate(flops=10**9, bytes_accessed=10**6, transcendentals=0),
    )(head_lambda, queries, out_first, out_second, cotangent, sums)
    keys_values = pl.pallas_call(
        pack_keys_kernel,
        out_shape=jax.ShapeDtypeStruct((n, 4 * DV), BF16),
        in_specs=vmem(3),
        out_specs=vmem(1)[0],
        cost_estimate=pl.CostEstimate(flops=10**9, bytes_accessed=3 * 10**6, transcendentals=0),
    )(key_vectors, latents, value_weight)

    blocks = [keys_values] + [lax.ppermute(keys_values, "y", ring(NY, -e)) for e in (1, 2, 3)]
    all_keys = jnp.concatenate(blocks, axis=0)
    ahead = [rows]
    behind = [rows]
    for _ in range(3):
        ahead.append(lax.ppermute(ahead[-1], "z", ring(NZ, -1)))
        behind.append(lax.ppermute(behind[-1], "z", ring(NZ, 1)))
    ahead.append(lax.ppermute(ahead[-1], "z", ring(NZ, -1)))

    source = {d: ahead[d] for d in range(5)} | {8 - d: behind[d] for d in (1, 2, 3)}
    acc = None
    returned = []
    own = None
    for index, offsets in enumerate(GROUPS):
        first, last = index == 0, index == len(GROUPS) - 1
        out = attention(offsets, first, last, zy, head_lambda, [source[d] for d in offsets], all_keys, acc)
        terms, acc = out[: len(offsets)], out[len(offsets) :]
        for d, term in zip(offsets, terms):
            if d == 0:
                own = term
            else:
                returned.append(lax.ppermute(term, "z", [(i, i + d) for i in range(NZ - d)]))
        if not last:
            acc = acc[0]
    value_parts, key_parts = acc[:NY], acc[NY:]
    value_parts = [value_parts[0]] + [lax.ppermute(value_parts[e], "y", ring(NY, e)) for e in (1, 2, 3)]
    key_parts = [key_parts[0]] + [lax.ppermute(key_parts[e], "y", ring(NY, e)) for e in (1, 2, 3)]

    rows_of_weight = latents.shape[1]
    call = pl.pallas_call(
        weight_term_kernel,
        out_shape=[
            jax.ShapeDtypeStruct((n, 2 * DV), BF16),
            jax.ShapeDtypeStruct((rows_of_weight, 2 * DV), BF16),
        ],
        in_specs=vmem(1 + NY),
        out_specs=vmem(2),
        cost_estimate=pl.CostEstimate(flops=10**9, bytes_accessed=3 * 10**6, transcendentals=0),
        compiler_params=pltpu.CompilerParams(vmem_limit_bytes=VMEM_LIMIT),
        name="weight_term",
    )
    values_grad, weight_term = call(latents, *value_parts)
    arrived_weight = lax.all_to_all(
        weight_term.reshape(NZ * NY, -1, 2 * DV), ("z", "y"), split_axis=0, concat_axis=0, tiled=True
    )
    size = lax.axis_size("tp")
    place = lax.axis_index("tp")
    side = jnp.stack([place // 2, place % 2]).astype(jnp.int32)
    columns = rows_of_weight // size
    smem = [pl.BlockSpec(memory_space=pltpu.SMEM)]
    kept, sent = pl.pallas_call(
        latent_term_kernel,
        out_shape=[jax.ShapeDtypeStruct((size // 2, n, columns), BF16)] * 2,
        in_specs=smem + vmem(2),
        out_specs=vmem(2),
        cost_estimate=pl.CostEstimate(flops=10**9, bytes_accessed=3 * 10**6, transcendentals=0),
        compiler_params=pltpu.CompilerParams(vmem_limit_bytes=VMEM_LIMIT),
        name="latent_term",
    )(side, values_grad, value_weight)
    arrived = lax.ppermute(sent, "tp", [(i, i ^ 1) for i in range(size)])
    latent_parts = pl.pallas_call(
        latent_pair_kernel,
        out_shape=[jax.ShapeDtypeStruct((n, columns), F32 if d == 0 else BF16) for d in range(size // 2)],
        in_specs=smem + vmem(2),
        out_specs=vmem(size // 2),
        cost_estimate=pl.CostEstimate(flops=10**8, bytes_accessed=10**6, transcendentals=0),
        compiler_params=pltpu.CompilerParams(vmem_limit_bytes=VMEM_LIMIT),
        name="latent_pair",
    )(side, kept, arrived)
    grad_latents = latent_parts[0]
    for d in range(1, size // 2):
        grad_latents = grad_latents + lax.ppermute(latent_parts[d], "tp", ring(size, 2 * d)).astype(F32)
    grad_latents = grad_latents.astype(BF16)

    grad_queries = own
    for term in returned:
        grad_queries = grad_queries + term.astype(F32)
    grad_queries = grad_queries * DH ** (-0.5)
    grad_keys = key_parts[0].astype(F32)
    for part in key_parts[1:]:
        grad_keys = grad_keys + part.astype(F32)
    grad_weight = arrived_weight.astype(F32).sum(axis=0)
    return (grad_queries, grad_keys, grad_latents, grad_weight)


def solution(mesh):
    devices = mesh.devices
    grid = jax.sharding.Mesh(devices.reshape(NZ, NY, devices.shape[1]), ("z", "y", "tp"))
    rows = ("z", "y")
    return jax.shard_map(
        program,
        mesh=grid,
        in_specs=(
            P(rows, "tp"),
            P(rows, "tp"),
            P(rows, None),
            P(None, "tp"),
            P(rows, "tp"),
            P(rows, "tp"),
            P(rows, "tp"),
            P(rows, "tp"),
            P("tp"),
        ),
        out_specs=(P(rows, "tp"), P(rows, "tp"), P(rows, "tp"), P(rows, "tp")),
        check_vma=False,
    )
```

time: 308 us -> 153 us (0.50)
  matrix products: 111 us -> 0 us
  local copies, waits for them, and re-layouts: 59.5 us -> 0.1 us
  starting transfers between devices: 7.41 us -> 63.6 us
  blocking collectives: 52.6 us -> 0 us
  Pallas kernels: 0 us -> 45 us
  between operations: 14 us -> 0.91 us
  waiting for transfers between devices: 46.8 us -> 34.8 us
  other arithmetic: 15.7 us -> 5.31 us
    dot_general x9 -> x0, matrix products: 111 us -> none  [the longest x1 24 us: block_grads(): jnp.einsum('hanm,mhad->nhad', d_scores, key_heads, preferred_element_type...]
    ppermute x0 -> x27, starting transfers between devices: none -> 56.9 us  [the longest x7 23.5 us: program(): lax.ppermute(term, 'z', [(i, i + d) for i in range(NZ - d)])]
    all_gather x1 -> x0, blocking collectives: 52.6 us -> none  [side_by_side(): out = lax.all_gather(both, axis, axis=dim, tiled=True)]
    all_gather x2 -> x0, waiting for transfers between devices: 46.8 us -> none  [side_by_side(): out = lax.all_gather(both, axis, axis=dim, tiled=True)]
    pallas_call x0 -> x10, Pallas kernels: none -> 45 us  [the longest x5 36.3 us: attention(): pl.pallas_call(functools.partial(attention_kernel, offsets, first_call, l...]
    another operation x9 -> x0, local copies, waits for them, and re-layouts: 38.9 us -> none
    ppermute x0 -> x27, waiting for transfers between devices: none -> 34.8 us  [the longest x7 21.9 us: program(): lax.ppermute(term, 'z', [(i, i + d) for i in range(NZ - d)])]
    split x5 -> x0, local copies, waits for them, and re-layouts: 15.4 us -> none  [side_by_side(): jnp.split(out, [sum(widths[:k]) for k in range(1, len(widths))], axis=along)]
  transfers between devices with their start and end apart: 4 -> 28, of which waited for: 1 -> 9; matrix products, arithmetic and copies ran while one was open for 57% -> 2% of each run, Pallas kernels for 0% -> 24%
where the time goes in v1:
time: 153 us; the launch traced here: 150 us
  starting transfers between devices  63.6 us (42%)
  Pallas kernels  45 us (29%)
  waiting for transfers between devices  34.8 us (23%)
  other arithmetic  5.31 us (3%)
    pallas_call x5, Pallas kernels, attention(): pl.pallas_call(functools.partial(attention_kernel, offsets, first_call, l...  36.3 us
    ppermute x7, starting transfers between devices, program(): lax.ppermute(term, 'z', [(i, i + d) for i in range(NZ - d)])  23.5 us
    ppermute x7, waiting for transfers between devices, program(): lax.ppermute(term, 'z', [(i, i + d) for i in range(NZ - d)])  21.9 us
    ppermute x4, starting transfers between devices, program(): ahead.append(lax.ppermute(ahead[-1], 'z', ring(NZ, -1)))  12.6 us
    all_to_all x1, starting transfers between devices, program(): lax.all_to_all(weight_term.reshape(NZ * NY, -1, 2 * DV), ('z', 'y'), spli...  6.77 us
    ppermute x3, starting transfers between devices, program(): lax.ppermute(latent_parts[d], 'tp', ring(size, 2 * d)).astype(F32)  5.75 us
    ppermute x3, waiting for transfers between devices, program(): lax.ppermute(value_parts[e], 'y', ring(NY, e))  5.54 us
    ppermute x3, starting transfers between devices, program(): lax.ppermute(value_parts[e], 'y', ring(NY, e))  5.51 us
  transfers between devices with their start and end apart: 28, of which 9 were waited for; matrix products, arithmetic and copies ran while one was open for 2% of the time, Pallas kernels for 24%

profile of v1, /device:TPU:8, one launch (start us, length us, event | category | flops | bytes accessed | tf_op | source)
XLA Modules:
  0.0 149.8 jit_solution(3055865261093644583)
XLA Ops:
  0.6 2.8 %shard_map.121 = bf16[288,512]{1,0:T(8,128)(2,1)} custom-call(bf16[288,256]{1,0:T(8,128)(2,1)} %key_ref.1, bf16[288,2048]{1,0:T(8,128)(2,1)} %latent_ref.3, bf16[2048,256]{1,0:T(8,128)(2,1)} %weight_ref.3), custom_call_target="tpu_custom_call" | custom-call | flops 1000000000 | bytes 3000000 | tf_op jit(solution)/shard_map/pallas_call | solution.py:232
  3.5 2.2 %collective-permute-start = (bf16[288,512]{1,0:T(8,128)(2,1)}, bf16[288,512]{1,0:T(8,128)(2,1)S(1)}, u32[]{:S(2)}, u32[]{:S(2)}) collective-permute-start(bf16[288,512]{1,0:T(8,128)(2,1)} %shard_map.121), channel_id=1, source_target_pairs={{0,24},{8,0},{16,8},{24,16},{1,25},{9,1},{17,9},{25,17},{2,26},{10... | collective-permute-start | bytes 884744 | tf_op jit(solution)/shard_map/ppermute | solution.py:240
  9.2 2.4 %shard_map.120.refs_0_ = bf16[304,512]{1,0:T(8,128)(2,1)} custom-call(f32[2]{0:T(128)} %lam_ref.11, bf16[288,256]{1,0:T(8,128)(2,1)} %q_ref.1, bf16[288,256]{1,0:T(8,128)(2,1)} %first_ref.1, bf16[288,256]{1,0:T(8,128)(2,1)} %second_ref.1, bf16[288,256]{1,0:T(8,128)(2,1)} %cot_ref.1, f32[16,288]{1,0:T(8,128)} %maximum_maximum_fusion.lse_ref), custom_call_target="tpu_custom_call" | custom-call | flops 1000000000 | bytes 1000000 | tf_op jit(solution)/shard_map/pallas_call | solution.py:225
  11.6 5.9 %collective-permute-start.3 = (bf16[304,512]{1,0:T(8,128)(2,1)}, bf16[304,512]{1,0:T(8,128)(2,1)S(1)}, u32[]{:S(2)}, u32[]{:S(2)}) collective-permute-start(bf16[304,512]{1,0:T(8,128)(2,1)} %shard_map.120.refs_0_), channel_id=1, source_target_pairs={{0,224},{32,0},{64,32},{96,64},{128,96},{160,128},{192,160},{224,1... | collective-permute-start | bytes 933896 | tf_op jit(solution)/shard_map/ppermute | solution.py:245
  17.5 2.3 %collective-permute-done.1 = bf16[288,512]{1,0:T(8,128)(2,1)S(1)} collective-permute-done((bf16[288,512]{1,0:T(8,128)(2,1)}, bf16[288,512]{1,0:T(8,128)(2,1)S(1)}, u32[]{:S(2)}, u32[]{:S(2)}) %collective-permute-start.1) | collective-permute-done | bytes 294944 | tf_op jit(solution)/shard_map/ppermute | solution.py:240
  20.7 5.0 %shard_map.122 = (f32[288,256]{1,0:T(8,128)S(1)}, f32[512,1152]{1,0:T(8,128)S(1)}) custom-call(s32[2]{0:T(128)S(1)} %pad_add_fusion.zy_ref, f32[2]{0:T(128)S(1)} %copy-done.3, bf16[304,512]{1,0:T(8,128)(2,1)S(1)} %copy-done.2, bf16[1152,512]{1,0:T(8,128)(2,1)S(1)} %pad_maximum_fusion.refs_1_.refs_2_), custom_call_target="tpu_custom_call" | custom-call | flops 4000000000 | bytes 1000000 | tf_op jit(solution)/shard_map/pallas_call | solution.py:201
  25.7 5.9 %collective-permute-start.7 = (bf16[304,512]{1,0:T(8,128)(2,1)S(1)}, bf16[304,512]{1,0:T(8,128)(2,1)S(1)}, u32[]{:S(2)}, u32[]{:S(2)}) collective-permute-start(bf16[304,512]{1,0:T(8,128)(2,1)S(1)} %collective-permute-done.3.refs_0_), channel_id=1, source_target_pairs={{0,224},{32,0},{64,32},{96,64},{128,96},{160,128},{192,160},{224,1... | collective-permute-start | bytes 933896 | tf_op jit(solution)/shard_map/ppermute | solution.py:245
  31.6 8.8 %shard_map.123 = (bf16[288,256]{1,0:T(8,128)(2,1)S(1)}, bf16[288,256]{1,0:T(8,128)(2,1)S(1)}, f32[512,1152]{1,0:T(8,128)S(1)}) custom-call(s32[2]{0:T(128)S(1)} %pad_add_fusion.zy_ref, f32[2]{0:T(128)S(1)} %copy-done.3, bf16[304,512]{1,0:T(8,128)(2,1)S(1)} %collective-permute-done.3.refs_0_, bf16[304,512]{1,0:T(8,128)(2,1)S(1)} %collective-permute-done.4.refs_1_, ...), custom_call_target="tpu_custom_call" | custom-call | flops 8000000000 | bytes 2000000 | tf_op jit(solution)/shard_map/pallas_call | solution.py:201
  42.5 8.6 %shard_map.124 = (bf16[288,256]{1,0:T(8,128)(2,1)S(1)}, bf16[288,256]{1,0:T(8,128)(2,1)S(1)}, f32[512,1152]{1,0:T(8,128)S(1)}) custom-call(s32[2]{0:T(128)S(1)} %pad_add_fusion.zy_ref, f32[2]{0:T(128)S(1)} %copy-done.3, bf16[304,512]{1,0:T(8,128)(2,1)S(1)} %collective-permute-done.7.refs_0_, bf16[304,512]{1,0:T(8,128)(2,1)S(1)} %collective-permute-done.8.refs_1_, ...), custom_call_target="tpu_custom_call" | custom-call | flops 8000000000 | bytes 2000000 | tf_op jit(solution)/shard_map/pallas_call | solution.py:201
  51.2 8.8 %shard_map.125 = (bf16[288,256]{1,0:T(8,128)(2,1)S(1)}, bf16[288,256]{1,0:T(8,128)(2,1)S(1)}, f32[512,1152]{1,0:T(8,128)S(1)}) custom-call(s32[2]{0:T(128)S(1)} %pad_add_fusion.zy_ref, f32[2]{0:T(128)S(1)} %copy-done.3, bf16[304,512]{1,0:T(8,128)(2,1)S(1)} %collective-permute-done.11.refs_0_, bf16[304,512]{1,0:T(8,128)(2,1)S(1)} %collective-permute-done.12.refs_1_, ...), custom_call_target="tpu_custom_call" | custom-call | flops 8000000000 | bytes 2000000 | tf_op jit(solution)/shard_map/pallas_call | solution.py:201
  60.1 5.1 %shard_map.126 = (bf16[288,256]{1,0:T(8,128)(2,1)S(1)}, bf16[288,256]{1,0:T(8,128)(2,1)S(1)}, bf16[288,256]{1,0:T(8,128)(2,1)S(1)}, bf16[288,256]{1,0:T(8,128)(2...) custom-call(s32[2]{0:T(128)S(1)} %pad_add_fusion.zy_ref, ...), custom_call_target="tpu_custom_call" | custom-call | flops 4000000000 | bytes 1000000 | tf_op jit(solution)/shard_map/pallas_call | solution.py:201
  67.2 3.5 %collective-permute-start.21 = (bf16[288,256]{1,0:T(8,128)(2,1)S(1)}, bf16[288,256]{1,0:T(8,128)(2,1)S(1)}, u32[]{:S(2)}, u32[]{:S(2)}) collective-permute-start(bf16[288,256]{1,0:T(8,128)(2,1)S(1)} %get-tuple-element.50), channel_id=1, source_target_pairs={{0,16},{8,24},{16,0},{24,8},{1,17},{9,25},{17,1},{25,9},{2,18},{10... | collective-permute-start | bytes 442376 | tf_op jit(solution)/shard_map/ppermute | solution.py:265
  70.7 2.2 %collective-permute-done.20.refs_1_ = bf16[288,256]{1,0:T(8,128)(2,1)S(1)} collective-permute-done((bf16[288,256]{1,0:T(8,128)(2,1)S(1)}, bf16[288,256]{1,0:T(8,128)(2,1)S(1)}, u32[]{:S(2)}, u32[]{:S(2)}) %collective-permute-start.20) | collective-permute-done | bytes 147488 | tf_op jit(solution)/shard_map/ppermute | solution.py:265
  78.0 6.8 %all-to-all-start = ((bf16[32,64,256]{2,1,0:T(8,128)(2,1)}), bf16[32,64,256]{2,1,0:T(8,128)(2,1)}, u32[]{:S(2)}, u32[]{:S(2)}) async-start(bf16[32,64,256]{2,1,0:T(8,128)(2,1)} %bitcast.5), calls=%async_computation | async-start | bytes 2097152 | tf_op jit(solution)/shard_map/all_to_all | solution.py:282
  86.1 3.4 %collective-permute-start.5 = (bf16[288,256]{1,0:T(8,128)(2,1)S(1)}, bf16[288,256]{1,0:T(8,128)(2,1)S(1)}, u32[]{:S(2)}, u32[]{:S(2)}) collective-permute-start(bf16[288,256]{1,0:T(8,128)(2,1)S(1)} %get-tuple-element.34), channel_id=1, source_target_pairs={{0,32},{32,64},{64,96},{96,128},{128,160},{160,192},{192,224},{1,3... | collective-permute-start | bytes 442376 | tf_op jit(solution)/shard_map/ppermute | solution.py:261
  89.5 2.6 %collective-permute-start.6 = (bf16[288,256]{1,0:T(8,128)(2,1)S(1)}, bf16[288,256]{1,0:T(8,128)(2,1)S(1)}, u32[]{:S(2)}, u32[]{:S(2)}) collective-permute-start(bf16[288,256]{1,0:T(8,128)(2,1)S(1)} %get-tuple-element.35), channel_id=1, source_target_pairs={{0,224},{1,225},{2,226},{3,227},{4,228},{5,229},{6,230},{7,231},{8... | collective-permute-start | bytes 442376 | tf_op jit(solution)/shard_map/ppermute | solution.py:261
  92.0 2.7 %collective-permute-start.10 = (bf16[288,256]{1,0:T(8,128)(2,1)S(1)}, bf16[288,256]{1,0:T(8,128)(2,1)S(1)}, u32[]{:S(2)}, u32[]{:S(2)}) collective-permute-start(bf16[288,256]{1,0:T(8,128)(2,1)S(1)} %get-tuple-element.38), channel_id=1, source_target_pairs={{0,192},{32,224},{1,193},{33,225},{2,194},{34,226},{3,195},{35,227... | collective-permute-start | bytes 442376 | tf_op jit(solution)/shard_map/ppermute | solution.py:261
  96.1 15.1 %collective-permute-done.5 = bf16[288,256]{1,0:T(8,128)(2,1)S(1)} collective-permute-done((bf16[288,256]{1,0:T(8,128)(2,1)S(1)}, bf16[288,256]{1,0:T(8,128)(2,1)S(1)}, u32[]{:S(2)}, u32[]{:S(2)}) %collective-permute-start.5) | collective-permute-done | bytes 147488 | tf_op jit(solution)/shard_map/ppermute | solution.py:261
  111.2 7.6 %collective-permute-start.13 = (bf16[288,256]{1,0:T(8,128)(2,1)S(1)}, bf16[288,256]{1,0:T(8,128)(2,1)S(1)}, u32[]{:S(2)}, u32[]{:S(2)}) collective-permute-start(bf16[288,256]{1,0:T(8,128)(2,1)S(1)} %get-tuple-element.40), channel_id=1, source_target_pairs={{0,96},{32,128},{64,160},{96,192},{128,224},{1,97},{33,129},{65,16... | collective-permute-start | bytes 442376 | tf_op jit(solution)/shard_map/ppermute | solution.py:261
  120.7 4.1 %collective-permute-start.16 = (bf16[288,256]{1,0:T(8,128)(2,1)S(1)}, bf16[288,256]{1,0:T(8,128)(2,1)S(1)}, u32[]{:S(2)}, u32[]{:S(2)}) collective-permute-start(bf16[288,256]{1,0:T(8,128)(2,1)S(1)} %get-tuple-element.43), channel_id=1, source_target_pairs={{0,128},{32,160},{64,192},{96,224},{1,129},{33,161},{65,193},{97,2... | collective-permute-start | bytes 442376 | tf_op jit(solution)/shard_map/ppermute | solution.py:261
  127.4 6.8 %collective-permute-done.14 = bf16[288,256]{1,0:T(8,128)(2,1)S(1)} collective-permute-done((bf16[288,256]{1,0:T(8,128)(2,1)S(1)}, bf16[288,256]{1,0:T(8,128)(2,1)S(1)}, u32[]{:S(2)}, u32[]{:S(2)}) %collective-permute-start.14) | collective-permute-done | bytes 147488 | tf_op jit(solution)/shard_map/ppermute | solution.py:261
  137.8 2.7 %collective-permute-start.25 = (bf16[288,256]{1,0:T(8,128)(2,1)S(1)}, bf16[288,256]{1,0:T(8,128)(2,1)S(1)}, u32[]{:S(2)}, u32[]{:S(2)}) collective-permute-start(bf16[288,256]{1,0:T(8,128)(2,1)S(1)} %get-tuple-element.57), channel_id=1, source_target_pairs={{0,4},{1,5},{2,6},{3,7},{4,0},{5,1},{6,2},{7,3},{8,12},{9,13},{10,... | collective-permute-start | bytes 442376 | tf_op jit(solution)/shard_map/ppermute | solution.py:311
  143.3 3.8 %collective-permute-done.25 = bf16[288,256]{1,0:T(8,128)(2,1)S(1)} collective-permute-done((bf16[288,256]{1,0:T(8,128)(2,1)S(1)}, bf16[288,256]{1,0:T(8,128)(2,1)S(1)}, u32[]{:S(2)}, u32[]{:S(2)}) %collective-permute-start.25) | collective-permute-done | bytes 147488 | tf_op jit(solution)/shard_map/ppermute | solution.py:311
  147.8 2.0 %convert_reduce_fusion = f32[64,256]{1,0:T(8,128)} fusion(bf16[32,64,256]{2,1,0:T(8,128)(2,1)} %all-to-all-done), kind=kLoop, calls=%fused_computation | loop fusion | flops 1032192 | bytes 1114112 | tf_op jit(solution)/shard_map/reduce_sum | solution.py:321
  (64 shorter events, 27.9 us)
Async XLA Ops:
  3.5 14.0 %collective-permute-start = (bf16[288,512]{1,0:T(8,128)(2,1)}, bf16[288,512]{1,0:T(8,128)(2,1)S(1)}, u32[]{:S(2)}, u32[]{:S(2)}) collective-permute-start(bf16[288,512]{1,0:T(8,128)(2,1)} %shard_map.121), channel_id=1, source_target_pairs={{0,24},{8,0},{16,8},{24,16},{1,25},{9,1},{17,9},{25,17},{2,26},{10... | collective-permute-start | bytes 884744 | tf_op jit(solution)/shard_map/ppermute | solution.py:240
  5.6 14.1 %collective-permute-start.1 = (bf16[288,512]{1,0:T(8,128)(2,1)}, bf16[288,512]{1,0:T(8,128)(2,1)S(1)}, u32[]{:S(2)}, u32[]{:S(2)}) collective-permute-start(bf16[288,512]{1,0:T(8,128)(2,1)} %shard_map.121), channel_id=1, source_target_pairs={{0,16},{8,24},{16,0},{24,8},{1,17},{9,25},{17,1},{25,9},{2,18},{10... | collective-permute-start | bytes 884744 | tf_op jit(solution)/shard_map/ppermute | solution.py:240
  6.5 14.1 %collective-permute-start.2 = (bf16[288,512]{1,0:T(8,128)(2,1)}, bf16[288,512]{1,0:T(8,128)(2,1)S(1)}, u32[]{:S(2)}, u32[]{:S(2)}) collective-permute-start(bf16[288,512]{1,0:T(8,128)(2,1)} %shard_map.121), channel_id=1, source_target_pairs={{0,8},{8,16},{16,24},{24,0},{1,9},{9,17},{17,25},{25,1},{2,10},{10... | collective-permute-start | bytes 884744 | tf_op jit(solution)/shard_map/ppermute | solution.py:240
  11.6 14.1 %collective-permute-start.3 = (bf16[304,512]{1,0:T(8,128)(2,1)}, bf16[304,512]{1,0:T(8,128)(2,1)S(1)}, u32[]{:S(2)}, u32[]{:S(2)}) collective-permute-start(bf16[304,512]{1,0:T(8,128)(2,1)} %shard_map.120.refs_0_), channel_id=1, source_target_pairs={{0,224},{32,0},{64,32},{96,64},{128,96},{160,128},{192,160},{224,1... | collective-permute-start | bytes 933896 | tf_op jit(solution)/shard_map/ppermute | solution.py:245
  17.4 14.2 %collective-permute-start.4 = (bf16[304,512]{1,0:T(8,128)(2,1)}, bf16[304,512]{1,0:T(8,128)(2,1)S(1)}, u32[]{:S(2)}, u32[]{:S(2)}) collective-permute-start(bf16[304,512]{1,0:T(8,128)(2,1)} %shard_map.120.refs_0_), channel_id=1, source_target_pairs={{0,32},{32,64},{64,96},{96,128},{128,160},{160,192},{192,224},{224... | collective-permute-start | bytes 933896 | tf_op jit(solution)/shard_map/ppermute | solution.py:246
  25.7 14.7 %collective-permute-start.7 = (bf16[304,512]{1,0:T(8,128)(2,1)S(1)}, bf16[304,512]{1,0:T(8,128)(2,1)S(1)}, u32[]{:S(2)}, u32[]{:S(2)}) collective-permute-start(bf16[304,512]{1,0:T(8,128)(2,1)S(1)} %collective-permute-done.3.refs_0_), channel_id=1, source_target_pairs={{0,224},{32,0},{64,32},{96,64},{128,96},{160,128},{192,160},{224,1... | collective-permute-start | bytes 933896 | tf_op jit(solution)/shard_map/ppermute | solution.py:245
  31.6 9.5 %collective-permute-start.8 = (bf16[304,512]{1,0:T(8,128)(2,1)S(1)}, bf16[304,512]{1,0:T(8,128)(2,1)S(1)}, u32[]{:S(2)}, u32[]{:S(2)}) collective-permute-start(bf16[304,512]{1,0:T(8,128)(2,1)S(1)} %collective-permute-done.4.refs_1_), channel_id=1, source_target_pairs={{0,32},{32,64},{64,96},{96,128},{128,160},{160,192},{192,224},{224... | collective-permute-start | bytes 933896 | tf_op jit(solution)/shard_map/ppermute | solution.py:246
  40.4 10.7 %collective-permute-start.11 = (bf16[304,512]{1,0:T(8,128)(2,1)S(1)}, bf16[304,512]{1,0:T(8,128)(2,1)S(1)}, u32[]{:S(2)}, u32[]{:S(2)}) collective-permute-start(bf16[304,512]{1,0:T(8,128)(2,1)S(1)} %collective-permute-done.7.refs_0_), channel_id=1, source_target_pairs={{0,224},{32,0},{64,32},{96,64},{128,96},{160,128},{192,160},{224,1... | collective-permute-start | bytes 933896 | tf_op jit(solution)/shard_map/ppermute | solution.py:245
  41.2 10.1 %collective-permute-start.12 = (bf16[304,512]{1,0:T(8,128)(2,1)S(1)}, bf16[304,512]{1,0:T(8,128)(2,1)S(1)}, u32[]{:S(2)}, u32[]{:S(2)}) collective-permute-start(bf16[304,512]{1,0:T(8,128)(2,1)S(1)} %collective-permute-done.8.refs_1_), channel_id=1, source_target_pairs={{0,32},{32,64},{64,96},{96,128},{128,160},{160,192},{192,224},{224... | collective-permute-start | bytes 933896 | tf_op jit(solution)/shard_map/ppermute | solution.py:246
  51.1 8.9 %collective-permute-start.15 = (bf16[304,512]{1,0:T(8,128)(2,1)S(1)}, bf16[304,512]{1,0:T(8,128)(2,1)S(1)}, u32[]{:S(2)}, u32[]{:S(2)}) collective-permute-start(bf16[304,512]{1,0:T(8,128)(2,1)S(1)} %collective-permute-done.11.refs_0_), channel_id=1, source_target_pairs={{0,224},{32,0},{64,32},{96,64},{128,96},{160,128},{192,160},{224,1... | collective-permute-start | bytes 933896 | tf_op jit(solution)/shard_map/ppermute | solution.py:247
  65.2 7.7 %collective-permute-start.20 = (bf16[288,256]{1,0:T(8,128)(2,1)S(1)}, bf16[288,256]{1,0:T(8,128)(2,1)S(1)}, u32[]{:S(2)}, u32[]{:S(2)}) collective-permute-start(bf16[288,256]{1,0:T(8,128)(2,1)S(1)} %get-tuple-element.49), channel_id=1, source_target_pairs={{0,8},{8,16},{16,24},{24,0},{1,9},{9,17},{17,25},{25,1},{2,10},{10... | collective-permute-start | bytes 442376 | tf_op jit(solution)/shard_map/ppermute | solution.py:265
  78.0 69.7 %all-to-all-start = ((bf16[32,64,256]{2,1,0:T(8,128)(2,1)}), bf16[32,64,256]{2,1,0:T(8,128)(2,1)}, u32[]{:S(2)}, u32[]{:S(2)}) async-start(bf16[32,64,256]{2,1,0:T(8,128)(2,1)} %bitcast.5), calls=%async_computation | async-start | bytes 2097152 | tf_op jit(solution)/shard_map/all_to_all | solution.py:282
  86.0 49.6 %collective-permute-start.23 = (bf16[4,288,256]{2,1,0:T(8,128)(2,1)S(1)}, bf16[4,288,256]{2,1,0:T(8,128)(2,1)S(1)}, u32[]{:S(2)}, u32[]{:S(2)}) collective-permute-start(bf16[4,288,256]{2,1,0:T(8,128)(2,1)S(1)} %get-tuple-element.54), channel_id=1, source_target_pairs={{0,1},{1,0},{2,3},{3,2},{4,5},{5,4},{6,7},{7,6},{8,9},{9,8},{10,11... | collective-permute-start | bytes 1769480 | tf_op jit(solution)/shard_map/ppermute | solution.py:299
  86.1 25.1 %collective-permute-start.5 = (bf16[288,256]{1,0:T(8,128)(2,1)S(1)}, bf16[288,256]{1,0:T(8,128)(2,1)S(1)}, u32[]{:S(2)}, u32[]{:S(2)}) collective-permute-start(bf16[288,256]{1,0:T(8,128)(2,1)S(1)} %get-tuple-element.34), channel_id=1, source_target_pairs={{0,32},{32,64},{64,96},{96,128},{128,160},{160,192},{192,224},{1,3... | collective-permute-start | bytes 442376 | tf_op jit(solution)/shard_map/ppermute | solution.py:261
  89.5 29.4 %collective-permute-start.6 = (bf16[288,256]{1,0:T(8,128)(2,1)S(1)}, bf16[288,256]{1,0:T(8,128)(2,1)S(1)}, u32[]{:S(2)}, u32[]{:S(2)}) collective-permute-start(bf16[288,256]{1,0:T(8,128)(2,1)S(1)} %get-tuple-element.35), channel_id=1, source_target_pairs={{0,224},{1,225},{2,226},{3,227},{4,228},{5,229},{6,230},{7,231},{8... | collective-permute-start | bytes 442376 | tf_op jit(solution)/shard_map/ppermute | solution.py:261
  92.0 28.7 %collective-permute-start.10 = (bf16[288,256]{1,0:T(8,128)(2,1)S(1)}, bf16[288,256]{1,0:T(8,128)(2,1)S(1)}, u32[]{:S(2)}, u32[]{:S(2)}) collective-permute-start(bf16[288,256]{1,0:T(8,128)(2,1)S(1)} %get-tuple-element.38), channel_id=1, source_target_pairs={{0,192},{32,224},{1,193},{33,225},{2,194},{34,226},{3,195},{35,227... | collective-permute-start | bytes 442376 | tf_op jit(solution)/shard_map/ppermute | solution.py:261
  94.8 30.0 %collective-permute-start.9 = (bf16[288,256]{1,0:T(8,128)(2,1)S(1)}, bf16[288,256]{1,0:T(8,128)(2,1)S(1)}, u32[]{:S(2)}, u32[]{:S(2)}) collective-permute-start(bf16[288,256]{1,0:T(8,128)(2,1)S(1)} %get-tuple-element.37), channel_id=1, source_target_pairs={{0,64},{32,96},{64,128},{96,160},{128,192},{160,224},{1,65},{33,97... | collective-permute-start | bytes 442376 | tf_op jit(solution)/shard_map/ppermute | solution.py:261
  111.2 14.4 %collective-permute-start.13 = (bf16[288,256]{1,0:T(8,128)(2,1)S(1)}, bf16[288,256]{1,0:T(8,128)(2,1)S(1)}, u32[]{:S(2)}, u32[]{:S(2)}) collective-permute-start(bf16[288,256]{1,0:T(8,128)(2,1)S(1)} %get-tuple-element.40), channel_id=1, source_target_pairs={{0,96},{32,128},{64,160},{96,192},{128,224},{1,97},{33,129},{65,16... | collective-permute-start | bytes 442376 | tf_op jit(solution)/shard_map/ppermute | solution.py:261
  118.9 15.3 %collective-permute-start.14 = (bf16[288,256]{1,0:T(8,128)(2,1)S(1)}, bf16[288,256]{1,0:T(8,128)(2,1)S(1)}, u32[]{:S(2)}, u32[]{:S(2)}) collective-permute-start(bf16[288,256]{1,0:T(8,128)(2,1)S(1)} %get-tuple-element.41), channel_id=1, source_target_pairs={{0,160},{32,192},{64,224},{1,161},{33,193},{65,225},{2,162},{34,19... | collective-permute-start | bytes 442376 | tf_op jit(solution)/shard_map/ppermute | solution.py:261
  120.7 14.0 %collective-permute-start.16 = (bf16[288,256]{1,0:T(8,128)(2,1)S(1)}, bf16[288,256]{1,0:T(8,128)(2,1)S(1)}, u32[]{:S(2)}, u32[]{:S(2)}) collective-permute-start(bf16[288,256]{1,0:T(8,128)(2,1)S(1)} %get-tuple-element.43), channel_id=1, source_target_pairs={{0,128},{32,160},{64,192},{96,224},{1,129},{33,161},{65,193},{97,2... | collective-permute-start | bytes 442376 | tf_op jit(solution)/shard_map/ppermute | solution.py:261
  124.8 15.7 %collective-permute-start.17 = (bf16[288,256]{1,0:T(8,128)(2,1)S(1)}, bf16[288,256]{1,0:T(8,128)(2,1)S(1)}, u32[]{:S(2)}, u32[]{:S(2)}) collective-permute-start(bf16[288,256]{1,0:T(8,128)(2,1)S(1)} %get-tuple-element.45), channel_id=1, source_target_pairs={{0,8},{8,16},{16,24},{24,0},{1,9},{9,17},{17,25},{25,1},{2,10},{10... | collective-permute-start | bytes 442376 | tf_op jit(solution)/shard_map/ppermute | solution.py:266
  125.6 16.3 %collective-permute-start.18 = (bf16[288,256]{1,0:T(8,128)(2,1)S(1)}, bf16[288,256]{1,0:T(8,128)(2,1)S(1)}, u32[]{:S(2)}, u32[]{:S(2)}) collective-permute-start(bf16[288,256]{1,0:T(8,128)(2,1)S(1)} %get-tuple-element.46), channel_id=1, source_target_pairs={{0,16},{8,24},{16,0},{24,8},{1,17},{9,25},{17,1},{25,9},{2,18},{10... | collective-permute-start | bytes 442376 | tf_op jit(solution)/shard_map/ppermute | solution.py:266
  134.2 7.8 %collective-permute-start.19 = (bf16[288,256]{1,0:T(8,128)(2,1)S(1)}, bf16[288,256]{1,0:T(8,128)(2,1)S(1)}, u32[]{:S(2)}, u32[]{:S(2)}) collective-permute-start(bf16[288,256]{1,0:T(8,128)(2,1)S(1)} %get-tuple-element.47), channel_id=1, source_target_pairs={{0,24},{8,0},{16,8},{24,16},{1,25},{9,1},{17,9},{25,17},{2,26},{10... | collective-permute-start | bytes 442376 | tf_op jit(solution)/shard_map/ppermute | solution.py:266
  137.8 9.2 %collective-permute-start.25 = (bf16[288,256]{1,0:T(8,128)(2,1)S(1)}, bf16[288,256]{1,0:T(8,128)(2,1)S(1)}, u32[]{:S(2)}, u32[]{:S(2)}) collective-permute-start(bf16[288,256]{1,0:T(8,128)(2,1)S(1)} %get-tuple-element.57), channel_id=1, source_target_pairs={{0,4},{1,5},{2,6},{3,7},{4,0},{5,1},{6,2},{7,3},{8,12},{9,13},{10,... | collective-permute-start | bytes 442376 | tf_op jit(solution)/shard_map/ppermute | solution.py:311
  (10 other events, 97.0 us)

commit v2 on v1

--- a/solution.py
+++ b/solution.py
@@ -13,7 +13,7 @@
 NZ = 8
 NY = 4
 STAT_ROWS = 16
-GROUPS = [(0,), (1, 7), (2, 6), (3, 5), (4,)]
+GROUPS = [(0,), (1, 7), (2, 6), (3, 4, 5)]
 VMEM_LIMIT = 24 * 2**20
 F32 = jnp.float32
 BF16 = jnp.bfloat16
@@ -69,6 +69,8 @@
     if not first_call:
         acc_in, refs = refs[0], refs[1:]
     dq_refs, refs = refs[:count], refs[count:]
+    if count > 2:
+        *refs, all_rows_ref, all_dq_ref = refs
     if last_call:
         total_refs, (acc_ref, kz_ref) = refs[: 2 * NY], refs[2 * NY :]
     else:
@@ -77,7 +79,8 @@
     n = width // NY
     z = zy_ref[0]
     y = zy_ref[1]
-    tile = 384 if width % 384 == 0 else 128
+    tiles = [width // 256 * 128, width - width // 256 * 128]
+    starts = [0, tiles[0]]
 
     low_lanes = lax.broadcasted_iota(jnp.int32, (1, DV), 1) < DH
     for h in range(2):
@@ -89,8 +92,10 @@
     else:
         acc_ref[...] = acc_in[...]
 
-    def cell(rows_ref, dq_ref, diagonal):
-        def head(h, carry):
+    def cells(rows_of, dq_of, live, diagonal):
+        def head(step, carry):
+            h = step % 2
+            rows_ref, dq_ref = rows_of(step // 2), dq_of(step // 2)
             cols = pl.ds(pl.multiple_of(h * DV, DV), DV)
             grad_cols = pl.ds(pl.multiple_of((h + 2) * DV, DV), DV)
             lam = lam_ref[h]
@@ -104,20 +109,24 @@
 
             def stat(row):
                 pick = jnp.where((piece_row == row) | (piece_row == row + 4), 1.0, 0.0)
-                return jnp.concatenate([dot(stats, pick.astype(BF16), TN)] * (tile // DV), axis=1)
+                return dot(stats, pick.astype(BF16), TN)
 
             lse0, lse1 = stat(2 * h), stat(2 * h + 1)
             dot0, dot1 = stat(2 * h + 8), stat(2 * h + 9)
             dq = jnp.zeros((n, DV), F32)
             both_q = jnp.concatenate([q0, q1], axis=0)
-            for t in range(width // tile):
-                span = slice(t * tile, (t + 1) * tile)
+            for start, tile in zip(starts, tiles):
+                span = slice(start, start + tile)
+
+                def wide(x):
+                    return jnp.concatenate([x] * (tile // DV), axis=1)
+
                 k = kv_ref[span, cols]
                 v = kv_ref[span, grad_cols]
-                s0 = dot(q0, k, NT) - lse0
-                s1 = dot(q1, k, NT) - lse1
+                s0 = dot(q0, k, NT) - wide(lse0)
+                s1 = dot(q1, k, NT) - wide(lse1)
                 if diagonal:
-                    key = lax.broadcasted_iota(jnp.int32, (1, tile), 1) + t * tile
+                    key = lax.broadcasted_iota(jnp.int32, (1, tile), 1) + start
                     block = (key >= n).astype(jnp.int32) + (key >= 2 * n).astype(jnp.int32) + (key >= 3 * n).astype(jnp.int32)
                     bound = jnp.where(block == 0, key, jnp.where(y + block >= NY, -1, n))
                     seen = lax.broadcasted_iota(jnp.int32, (n, tile), 0) >= bound
@@ -126,8 +135,8 @@
                 p0 = jnp.exp(s0)
                 p1 = lam * jnp.exp(s1)
                 d_attn = dot(g, v, NT)
-                ds0 = (p0 * (d_attn - dot0)).astype(BF16)
-                ds1 = (p1 * (dot1 - d_attn)).astype(BF16)
+                ds0 = (p0 * (d_attn - wide(dot0))).astype(BF16)
+                ds1 = (p1 * (wide(dot1) - d_attn)).astype(BF16)
                 weights = (p0 - p1).astype(BF16)
                 dq = dq + dot(ds0, kz_ref[2 * h, span, :]) + dot(ds1, kz_ref[2 * h + 1, span, :])
                 both_ds = jnp.concatenate([ds0, ds1], axis=0)
@@ -136,13 +145,18 @@
             dq_ref[:, cols] = dq.astype(dq_ref.dtype)
             return carry
 
-        lax.fori_loop(0, 2, head, 0)
-
-    for rows_ref, dq_ref, offset in zip(row_refs, dq_refs, offsets):
-        if offset == 0:
-            cell(rows_ref, dq_ref, True)
-        else:
-            pl.when(z + offset < NZ)(functools.partial(cell, rows_ref, dq_ref, False))
+        lax.fori_loop(0, 2 * live, head, 0)
+
+    live = [(z + offset < NZ).astype(jnp.int32) for offset in offsets]
+    if count < 3:
+        for i, offset in enumerate(offsets):
+            cells(lambda _, i=i: row_refs[i], lambda _, i=i: dq_refs[i], live[i], offset == 0)
+    else:
+        for i, rows_ref in enumerate(row_refs):
+            all_rows_ref[i] = rows_ref[...]
+        cells(all_rows_ref.at.__getitem__, all_dq_ref.at.__getitem__, sum(live), False)
+        for i, dq_ref in enumerate(dq_refs):
+            dq_ref[...] = all_dq_ref[i]
     if last_call:
         for t in range(width // DV):
             turned = acc_ref[:, t * DV : (t + 1) * DV].T.astype(BF16)
@@ -156,6 +170,16 @@
                 start = stop
 
 
+def sum_kernel(scale, *refs):
+    *part_refs, out_ref = refs
+    total = part_refs[0][...].astype(F32)
+    for part in part_refs[1:]:
+        total = total + part[...].astype(F32)
+    if scale != 1.0:
+        total = total * scale
+    out_ref[...] = total.astype(out_ref.dtype)
+
+
 def weight_term_kernel(latent_ref, *refs):
     *part_refs, grad_ref, out_ref = refs
     total = part_refs[0][...].astype(F32)
@@ -197,6 +221,8 @@
     scratch = [pltpu.VMEM((4, width, DV), BF16)]
     if last_call:
         scratch = [pltpu.VMEM((4 * DV, width), F32)] + scratch
+    if count > 2:
+        scratch += [pltpu.VMEM((count, n + STAT_ROWS, 4 * DV), BF16), pltpu.VMEM((count, n, 2 * DV), BF16)]
     smem = [pl.BlockSpec(memory_space=pltpu.SMEM)] * 2
     return pl.pallas_call(
         functools.partial(attention_kernel, offsets, first_call, last_call),
@@ -207,6 +233,25 @@
         cost_estimate=pl.CostEstimate(flops=count * 4 * 10**9, bytes_accessed=count * 10**6, transcendentals=0),
         compiler_params=pltpu.CompilerParams(vmem_limit_bytes=VMEM_LIMIT),
     )(*operands)
+
+
+def gather_kernel(parts_ref, out_ref):
+    total = parts_ref[0].astype(F32)
+    for i in range(1, parts_ref.shape[0]):
+        total = total + parts_ref[i].astype(F32)
+    out_ref[...] = total
+
+
+def added(parts, dtype, scale=1.0):
+    return pl.pallas_call(
+        functools.partial(sum_kernel, scale),
+        out_shape=jax.ShapeDtypeStruct(parts[0].shape, dtype),
+        in_specs=vmem(len(parts)),
+        out_specs=vmem(1)[0],
+        cost_estimate=pl.CostEstimate(flops=10**8, bytes_accessed=10**6, transcendentals=0),
+        compiler_params=pltpu.CompilerParams(vmem_limit_bytes=VMEM_LIMIT),
+        name="added",
+    )(*parts)
 
 
 def ring(size, step):
@@ -237,18 +282,23 @@
         cost_estimate=pl.CostEstimate(flops=10**9, bytes_accessed=3 * 10**6, transcendentals=0),
     )(key_vectors, latents, value_weight)
 
-    blocks = [keys_values] + [lax.ppermute(keys_values, "y", ring(NY, -e)) for e in (1, 2, 3)]
-    all_keys = jnp.concatenate(blocks, axis=0)
+    half = n // 2
+    after = lax.ppermute(keys_values, "y", ring(NY, -1))
+    before = lax.ppermute(keys_values, "y", ring(NY, 1))
+    upper = lax.ppermute(after[:half], "y", ring(NY, -1))
+    lower = lax.ppermute(before[half:], "y", ring(NY, 1))
+    all_keys = jnp.concatenate([keys_values, after, upper, lower, before], axis=0)
     ahead = [rows]
     behind = [rows]
-    for _ in range(3):
-        ahead.append(lax.ppermute(ahead[-1], "z", ring(NZ, -1)))
-        behind.append(lax.ppermute(behind[-1], "z", ring(NZ, 1)))
-    ahead.append(lax.ppermute(ahead[-1], "z", ring(NZ, -1)))
-
+    for t in range(1, 5):
+        ahead.append(lax.ppermute(ahead[-1], "z", [(k + 1, k) for k in range(NZ - t)]))
+        if t < 4:
+            behind.append(lax.ppermute(behind[-1], "z", [((k + t + 4) % NZ, (k + t + 5) % NZ) for k in range(3)]))
+    smem = [pl.BlockSpec(memory_space=pltpu.SMEM)]
     source = {d: ahead[d] for d in range(5)} | {8 - d: behind[d] for d in (1, 2, 3)}
     acc = None
     returned = []
+    parts = {}
     own = None
     for index, offsets in enumerate(GROUPS):
         first, last = index == 0, index == len(GROUPS) - 1
@@ -258,10 +308,15 @@
             if d == 0:
                 own = term
             else:
-                returned.append(lax.ppermute(term, "z", [(i, i + d) for i in range(NZ - d)]))
+                parts[d] = term
+                if d < 3 or d > 4:
+                    returned.append(lax.ppermute(term, "z", [(i, i + d) for i in range(NZ - d)]))
         if not last:
             acc = acc[0]
     value_parts, key_parts = acc[:NY], acc[NY:]
+    hop = lax.ppermute(parts[4], "z", [(i, i + 1) for i in range(NZ - 4)])
+    joined = added([parts[3], hop], BF16)
+    returned.append(lax.ppermute(joined, "z", [(i, i + 3) for i in range(NZ - 3)]))
     value_parts = [value_parts[0]] + [lax.ppermute(value_parts[e], "y", ring(NY, e)) for e in (1, 2, 3)]
     key_parts = [key_parts[0]] + [lax.ppermute(key_parts[e], "y", ring(NY, e)) for e in (1, 2, 3)]
 
@@ -286,7 +341,6 @@
     place = lax.axis_index("tp")
     side = jnp.stack([place // 2, place % 2]).astype(jnp.int32)
     columns = rows_of_weight // size
-    smem = [pl.BlockSpec(memory_space=pltpu.SMEM)]
     kept, sent = pl.pallas_call(
         latent_term_kernel,
         out_shape=[jax.ShapeDtypeStruct((size // 2, n, columns), BF16)] * 2,
@@ -297,7 +351,7 @@
         name="latent_term",
     )(side, values_grad, value_weight)
     arrived = lax.ppermute(sent, "tp", [(i, i ^ 1) for i in range(size)])
-    latent_parts = pl.pallas_call(
+    call = pl.pallas_call(
         latent_pair_kernel,
         out_shape=[jax.ShapeDtypeStruct((n, columns), F32 if d == 0 else BF16) for d in range(size // 2)],
         in_specs=smem + vmem(2),
@@ -305,20 +359,24 @@
         cost_estimate=pl.CostEstimate(flops=10**8, bytes_accessed=10**6, transcendentals=0),
         compiler_params=pltpu.CompilerParams(vmem_limit_bytes=VMEM_LIMIT),
         name="latent_pair",
-    )(side, kept, arrived)
+    )
+    latent_parts = call(side, kept, arrived)
     grad_latents = latent_parts[0]
     for d in range(1, size // 2):
         grad_latents = grad_latents + lax.ppermute(latent_parts[d], "tp", ring(size, 2 * d)).astype(F32)
     grad_latents = grad_latents.astype(BF16)
 
-    grad_queries = own
-    for term in returned:
-        grad_queries = grad_queries + term.astype(F32)
-    grad_queries = grad_queries * DH ** (-0.5)
-    grad_keys = key_parts[0].astype(F32)
-    for part in key_parts[1:]:
-        grad_keys = grad_keys + part.astype(F32)
-    grad_weight = arrived_weight.astype(F32).sum(axis=0)
+    grad_queries = added([own, *returned], F32, DH ** (-0.5))
+    grad_keys = added(key_parts, F32)
+    grad_weight = pl.pallas_call(
+        gather_kernel,
+        out_shape=jax.ShapeDtypeStruct(arrived_weight.shape[1:], F32),
+        in_specs=vmem(1),
+        out_specs=vmem(1)[0],
+        cost_estimate=pl.CostEstimate(flops=10**8, bytes_accessed=10**6, transcendentals=0),
+        compiler_params=pltpu.CompilerParams(vmem_limit_bytes=VMEM_LIMIT),
+        name="weight_sum",
+    )(arrived_weight)
     return (grad_queries, grad_keys, grad_latents, grad_weight)
 
 

time: 153 us -> 148 us (0.967)
  the two profiles are of different devices: /device:TPU:8 before, /device:TPU:56 now
where the time goes in v2:
time: 148 us; the launch traced here: 147 us
  starting transfers between devices  70 us (47%)
  Pallas kernels  40.6 us (27%)
  waiting for transfers between devices  31 us (21%)
  local copies, waits for them, and re-layouts  3.13 us (2%)
  other arithmetic  1.57 us (1%)
    pallas_call x4, Pallas kernels, attention(): pl.pallas_call(functools.partial(attention_kernel, offsets, first_call, l...  29.4 us
    ppermute x5, starting transfers between devices, program(): lax.ppermute(term, 'z', [(i, i + d) for i in range(NZ - d)])  26.1 us
    ppermute x4, starting transfers between devices, program(): lax.ppermute(ahead[-1], 'z', [(k + 1, k) for k in range(NZ - t)])  14.3 us
    ppermute x5, waiting for transfers between devices, program(): lax.ppermute(term, 'z', [(i, i + d) for i in range(NZ - d)])  12.8 us
    ppermute x3, waiting for transfers between devices, program(): lax.ppermute(value_parts[e], 'y', ring(NY, e))  6.99 us
    all_to_all x1, starting transfers between devices, program(): lax.all_to_all(weight_term.reshape(NZ * NY, -1, 2 * DV), ('z', 'y'), spli...  5.7 us
    ppermute x4, waiting for transfers between devices, program(): lax.ppermute(ahead[-1], 'z', [(k + 1, k) for k in range(NZ - t)])  5.32 us
    ppermute x3, waiting for transfers between devices, program(): lax.ppermute(latent_parts[d], 'tp', ring(size, 2 * d)).astype(F32)  4.89 us
  transfers between devices with their start and end apart: 29, of which 11 were waited for; matrix products, arithmetic and copies ran while one was open for 1% of the time, Pallas kernels for 16%

profile of v2, /device:TPU:56, one launch (start us, length us, event | category | flops | bytes accessed | tf_op | source)
XLA Modules:
  0.0 147.4 jit_solution(6248111562967255721)
XLA Ops:
  0.6 2.8 %shard_map.121 = bf16[288,512]{1,0:T(8,128)(2,1)} custom-call(bf16[288,256]{1,0:T(8,128)(2,1)} %key_ref.1, bf16[288,2048]{1,0:T(8,128)(2,1)} %latent_ref.3, bf16[2048,256]{1,0:T(8,128)(2,1)} %weight_ref.3), custom_call_target="tpu_custom_call" | custom-call | flops 1000000000 | bytes 3000000 | tf_op jit(solution)/shard_map/pallas_call | solution.py:277
  4.2 2.5 %collective-permute-start.2 = (bf16[288,512]{1,0:T(8,128)(2,1)}, bf16[288,512]{1,0:T(8,128)(2,1)S(1)}, u32[]{:S(2)}, u32[]{:S(2)}) collective-permute-start(bf16[288,512]{1,0:T(8,128)(2,1)} %shard_map.121), channel_id=1, source_target_pairs={{0,8},{8,16},{16,24},{24,0},{1,9},{9,17},{17,25},{25,1},{2,10},{10... | collective-permute-start | bytes 884744 | tf_op jit(solution)/shard_map/ppermute | solution.py:287
  7.5 2.4 %shard_map.120.refs_0_ = bf16[304,512]{1,0:T(8,128)(2,1)} custom-call(f32[2]{0:T(128)} %lam_ref.9, bf16[288,256]{1,0:T(8,128)(2,1)} %q_ref.1, bf16[288,256]{1,0:T(8,128)(2,1)} %first_ref.1, bf16[288,256]{1,0:T(8,128)(2,1)} %second_ref.1, bf16[288,256]{1,0:T(8,128)(2,1)} %cot_ref.1, f32[16,288]{1,0:T(8,128)} %maximum_maximum_fusion.lse_ref), custom_call_target="tpu_custom_call" | custom-call | flops 1000000000 | bytes 1000000 | tf_op jit(solution)/shard_map/pallas_call | solution.py:270
  9.9 2.0 %collective-permute-start.4 = (bf16[304,512]{1,0:T(8,128)(2,1)}, bf16[304,512]{1,0:T(8,128)(2,1)S(1)}, u32[]{:S(2)}, u32[]{:S(2)}) collective-permute-start(bf16[304,512]{1,0:T(8,128)(2,1)} %shard_map.120.refs_0_), channel_id=1, source_target_pairs={{32,0},{64,32},{96,64},{128,96},{160,128},{192,160},{224,192},{33,... | collective-permute-start | bytes 933896 | tf_op jit(solution)/shard_map/ppermute | solution.py:294
  13.8 3.3 %collective-permute-start.3 = (bf16[144,512]{1,0:T(8,128)(2,1)S(1)}, bf16[144,512]{1,0:T(8,128)(2,1)S(1)}, u32[]{:S(2)}, u32[]{:S(2)}) collective-permute-start(bf16[144,512]{1,0:T(8,128)(2,1)S(1)} %slice.9), channel_id=1, source_target_pairs={{0,8},{8,16},{16,24},{24,0},{1,9},{9,17},{17,25},{25,1},{2,10},{10... | collective-permute-start | bytes 442376 | tf_op jit(solution)/shard_map/ppermute | solution.py:289
  17.1 3.5 %collective-permute-done.4.refs_0_ = bf16[304,512]{1,0:T(8,128)(2,1)S(1)} collective-permute-done((bf16[304,512]{1,0:T(8,128)(2,1)}, bf16[304,512]{1,0:T(8,128)(2,1)S(1)}, u32[]{:S(2)}, u32[]{:S(2)}) %collective-permute-start.4) | collective-permute-done | bytes 311328 | tf_op jit(solution)/shard_map/ppermute | solution.py:294
  24.1 4.7 %shard_map.122 = (f32[288,256]{1,0:T(8,128)S(1)}, f32[512,1152]{1,0:T(8,128)S(1)}) custom-call(s32[2]{0:T(128)S(1)} %pad_add_fusion.zy_ref, f32[2]{0:T(128)S(1)} %copy-done.11, bf16[304,512]{1,0:T(8,128)(2,1)S(1)} %copy-done.2, bf16[1152,512]{1,0:T(8,128)(2,1)S(1)} %constant_dynamic-update-slice_fusion.refs_1_.refs_2_.refs_3_), custom_call_target="tpu_custom_call" | custom-call | flops 4000000000 | bytes 1000000 | tf_op jit(solution)/shard_map/pallas_call | solution.py:227
  30.6 5.4 %collective-permute-start.12 = (bf16[304,512]{1,0:T(8,128)(2,1)S(1)}, bf16[304,512]{1,0:T(8,128)(2,1)S(1)}, u32[]{:S(2)}, u32[]{:S(2)}) collective-permute-start(bf16[304,512]{1,0:T(8,128)(2,1)S(1)} %collective-permute-done.8.refs_0_), channel_id=1, source_target_pairs={{32,0},{64,32},{96,64},{128,96},{160,128},{33,1},{65,33},{97,65},{... | collective-permute-start | bytes 933896 | tf_op jit(solution)/shard_map/ppermute | solution.py:294
  36.1 4.5 %shard_map.123 = (bf16[288,256]{1,0:T(8,128)(2,1)S(1)}, bf16[288,256]{1,0:T(8,128)(2,1)S(1)}, f32[512,1152]{1,0:T(8,128)S(1)}) custom-call(s32[2]{0:T(128)S(1)} %pad_add_fusion.zy_ref, f32[2]{0:T(128)S(1)} %copy-done.11, bf16[304,512]{1,0:T(8,128)(2,1)S(1)} %collective-permute-done.4.refs_0_, bf16[304,512]{1,0:T(8,128)(2,1)S(1)} %collective-permute-done.5.refs_1_, ...), custom_call_target="tpu_custom_call" | custom-call | flops 8000000000 | bytes 2000000 | tf_op jit(solution)/shard_map/pallas_call | solution.py:227
  43.2 4.8 %collective-permute-start.13 = (bf16[304,512]{1,0:T(8,128)(2,1)S(1)}, bf16[304,512]{1,0:T(8,128)(2,1)S(1)}, u32[]{:S(2)}, u32[]{:S(2)}) collective-permute-start(bf16[304,512]{1,0:T(8,128)(2,1)S(1)} %collective-permute-done.12.refs_0_), channel_id=1, source_target_pairs={{32,0},{64,32},{96,64},{128,96},{33,1},{65,33},{97,65},{129,97},{3... | collective-permute-start | bytes 933896 | tf_op jit(solution)/shard_map/ppermute | solution.py:294
  48.0 8.2 %shard_map.124 = (bf16[288,256]{1,0:T(8,128)(2,1)S(1)}, bf16[288,256]{1,0:T(8,128)(2,1)S(1)}, f32[512,1152]{1,0:T(8,128)S(1)}) custom-call(s32[2]{0:T(128)S(1)} %pad_add_fusion.zy_ref, f32[2]{0:T(128)S(1)} %copy-done.11, bf16[304,512]{1,0:T(8,128)(2,1)S(1)} %collective-permute-done.8.refs_0_, bf16[304,512]{1,0:T(8,128)(2,1)S(1)} %collective-permute-done.9.refs_1_, ...), custom_call_target="tpu_custom_call" | custom-call | flops 8000000000 | bytes 2000000 | tf_op jit(solution)/shard_map/pallas_call | solution.py:227
  56.8 12.0 %shard_map.125 = (bf16[288,256]{1,0:T(8,128)(2,1)S(1)}, bf16[288,256]{1,0:T(8,128)(2,1)S(1)}, bf16[288,256]{1,0:T(8,128)(2,1)S(1)}, bf16[288,256]{1,0:T(8,128)(2...) custom-call(s32[2]{0:T(128)S(1)} %pad_add_fusion.zy_ref, ...), custom_call_target="tpu_custom_call" | custom-call | flops 12000000000 | bytes 3000000 | tf_op jit(solution)/shard_map/pallas_call | solution.py:227
  71.0 3.4 %collective-permute-done.21.refs_1_ = bf16[288,256]{1,0:T(8,128)(2,1)S(1)} collective-permute-done((bf16[288,256]{1,0:T(8,128)(2,1)S(1)}, bf16[288,256]{1,0:T(8,128)(2,1)S(1)}, u32[]{:S(2)}, u32[]{:S(2)}) %collective-permute-start.21) | collective-permute-done | bytes 147488 | tf_op jit(solution)/shard_map/ppermute | solution.py:320
  74.4 2.1 %collective-permute-done.22.refs_2_ = bf16[288,256]{1,0:T(8,128)(2,1)S(1)} collective-permute-done((bf16[288,256]{1,0:T(8,128)(2,1)S(1)}, bf16[288,256]{1,0:T(8,128)(2,1)S(1)}, u32[]{:S(2)}, u32[]{:S(2)}) %collective-permute-start.22) | collective-permute-done | bytes 147488 | tf_op jit(solution)/shard_map/ppermute | solution.py:320
  80.4 5.7 %all-to-all-start = ((bf16[32,64,256]{2,1,0:T(8,128)(2,1)}), bf16[32,64,256]{2,1,0:T(8,128)(2,1)S(1)}, u32[]{:S(2)}, u32[]{:S(2)}) async-start(bf16[32,64,256]{2,1,0:T(8,128)(2,1)} %bitcast.5), calls=%async_computation | async-start | bytes 2097152 | tf_op jit(solution)/shard_map/all_to_all | solution.py:337
  88.3 3.4 %collective-permute-start.6 = (bf16[288,256]{1,0:T(8,128)(2,1)S(1)}, bf16[288,256]{1,0:T(8,128)(2,1)S(1)}, u32[]{:S(2)}, u32[]{:S(2)}) collective-permute-start(bf16[288,256]{1,0:T(8,128)(2,1)S(1)} %copy-done.6), channel_id=1, source_target_pairs={{0,32},{32,64},{64,96},{96,128},{128,160},{160,192},{192,224},{1,3... | collective-permute-start | bytes 442376 | tf_op jit(solution)/shard_map/ppermute | solution.py:313
  92.4 5.5 %collective-permute-start.10 = (bf16[288,256]{1,0:T(8,128)(2,1)S(1)}, bf16[288,256]{1,0:T(8,128)(2,1)S(1)}, u32[]{:S(2)}, u32[]{:S(2)}) collective-permute-start(bf16[288,256]{1,0:T(8,128)(2,1)S(1)} %copy-done.8), channel_id=1, source_target_pairs={{0,64},{32,96},{64,128},{96,160},{128,192},{160,224},{1,65},{33,97... | collective-permute-start | bytes 442376 | tf_op jit(solution)/shard_map/ppermute | solution.py:313
  97.9 2.5 %collective-permute-start.16 = (bf16[288,256]{1,0:T(8,128)(2,1)S(1)}, bf16[288,256]{1,0:T(8,128)(2,1)S(1)}, u32[]{:S(2)}, u32[]{:S(2)}) collective-permute-start(bf16[288,256]{1,0:T(8,128)(2,1)S(1)} %copy-done.10), channel_id=1, source_target_pairs={{0,32},{32,64},{64,96},{96,128},{1,33},{33,65},{65,97},{97,129},{2... | collective-permute-start | bytes 442376 | tf_op jit(solution)/shard_map/ppermute | solution.py:317
  100.4 12.4 %collective-permute-done.6.refs_1_ = bf16[288,256]{1,0:T(8,128)(2,1)S(1)} collective-permute-done((bf16[288,256]{1,0:T(8,128)(2,1)S(1)}, bf16[288,256]{1,0:T(8,128)(2,1)S(1)}, u32[]{:S(2)}, u32[]{:S(2)}) %collective-permute-start.6) | collective-permute-done | bytes 147488 | tf_op jit(solution)/shard_map/ppermute | solution.py:313
  112.8 3.0 %collective-permute-start.11 = (bf16[288,256]{1,0:T(8,128)(2,1)S(1)}, bf16[288,256]{1,0:T(8,128)(2,1)S(1)}, u32[]{:S(2)}, u32[]{:S(2)}) collective-permute-start(bf16[288,256]{1,0:T(8,128)(2,1)S(1)} %get-tuple-element.37), channel_id=1, source_target_pairs={{0,192},{32,224},{1,193},{33,225},{2,194},{34,226},{3,195},{35,227... | collective-permute-start | bytes 442376 | tf_op jit(solution)/shard_map/ppermute | solution.py:313
  116.7 2.3 %collective-permute-start.19 = (bf16[288,256]{1,0:T(8,128)(2,1)S(1)}, bf16[288,256]{1,0:T(8,128)(2,1)S(1)}, u32[]{:S(2)}, u32[]{:S(2)}) collective-permute-start(bf16[288,256]{1,0:T(8,128)(2,1)S(1)} %get-tuple-element.44), channel_id=1, source_target_pairs={{0,16},{8,24},{16,0},{24,8},{1,17},{9,25},{17,1},{25,9},{2,18},{10... | collective-permute-start | bytes 442376 | tf_op jit(solution)/shard_map/ppermute | solution.py:321
  119.3 13.5 %collective-permute-start.15 = (bf16[288,256]{1,0:T(8,128)(2,1)S(1)}, bf16[288,256]{1,0:T(8,128)(2,1)S(1)}, u32[]{:S(2)}, u32[]{:S(2)}) collective-permute-start(bf16[288,256]{1,0:T(8,128)(2,1)S(1)} %get-tuple-element.39), channel_id=1, source_target_pairs={{0,160},{32,192},{64,224},{1,161},{33,193},{65,225},{2,162},{34,19... | collective-permute-start | bytes 442376 | tf_op jit(solution)/shard_map/ppermute | solution.py:313
  134.8 2.9 %collective-permute-start.27 = (bf16[288,256]{1,0:T(8,128)(2,1)S(1)}, bf16[288,256]{1,0:T(8,128)(2,1)S(1)}, u32[]{:S(2)}, u32[]{:S(2)}) collective-permute-start(bf16[288,256]{1,0:T(8,128)(2,1)S(1)} %get-tuple-element.56), channel_id=1, source_target_pairs={{0,6},{1,7},{2,0},{3,1},{4,2},{5,3},{6,4},{7,5},{8,14},{9,15},{10,... | collective-permute-start | bytes 442376 | tf_op jit(solution)/shard_map/ppermute | solution.py:366
  141.9 2.5 %collective-permute-done.26 = bf16[288,256]{1,0:T(8,128)(2,1)S(1)} collective-permute-done((bf16[288,256]{1,0:T(8,128)(2,1)S(1)}, bf16[288,256]{1,0:T(8,128)(2,1)S(1)}, u32[]{:S(2)}, u32[]{:S(2)}) %collective-permute-start.26) | collective-permute-done | bytes 147488 | tf_op jit(solution)/shard_map/ppermute | solution.py:366
  (92 shorter events, 31.0 us)
Async XLA Ops:
  3.5 10.2 %collective-permute-start = (bf16[288,512]{1,0:T(8,128)(2,1)}, bf16[288,512]{1,0:T(8,128)(2,1)S(1)}, u32[]{:S(2)}, u32[]{:S(2)}) collective-permute-start(bf16[288,512]{1,0:T(8,128)(2,1)} %shard_map.121), channel_id=1, source_target_pairs={{0,24},{8,0},{16,8},{24,16},{1,25},{9,1},{17,9},{25,17},{2,26},{10... | collective-permute-start | bytes 884744 | tf_op jit(solution)/shard_map/ppermute | solution.py:286
  4.2 9.6 %collective-permute-start.2 = (bf16[288,512]{1,0:T(8,128)(2,1)}, bf16[288,512]{1,0:T(8,128)(2,1)S(1)}, u32[]{:S(2)}, u32[]{:S(2)}) collective-permute-start(bf16[288,512]{1,0:T(8,128)(2,1)} %shard_map.121), channel_id=1, source_target_pairs={{0,8},{8,16},{16,24},{24,0},{1,9},{9,17},{17,25},{25,1},{2,10},{10... | collective-permute-start | bytes 884744 | tf_op jit(solution)/shard_map/ppermute | solution.py:287
  9.9 10.8 %collective-permute-start.4 = (bf16[304,512]{1,0:T(8,128)(2,1)}, bf16[304,512]{1,0:T(8,128)(2,1)S(1)}, u32[]{:S(2)}, u32[]{:S(2)}) collective-permute-start(bf16[304,512]{1,0:T(8,128)(2,1)} %shard_map.120.refs_0_), channel_id=1, source_target_pairs={{32,0},{64,32},{96,64},{128,96},{160,128},{192,160},{224,192},{33,... | collective-permute-start | bytes 933896 | tf_op jit(solution)/shard_map/ppermute | solution.py:294
  11.9 10.8 %collective-permute-start.5 = (bf16[304,512]{1,0:T(8,128)(2,1)}, bf16[304,512]{1,0:T(8,128)(2,1)S(1)}, u32[]{:S(2)}, u32[]{:S(2)}) collective-permute-start(bf16[304,512]{1,0:T(8,128)(2,1)} %shard_map.120.refs_0_), channel_id=1, source_target_pairs={{160,192},{192,224},{224,0},{161,193},{193,225},{225,1},{162,194},... | collective-permute-start | bytes 933896 | tf_op jit(solution)/shard_map/ppermute | solution.py:296
  13.6 10.4 %collective-permute-start.1 = (bf16[144,512]{1,0:T(8,128)(2,1)S(1)}, bf16[144,512]{1,0:T(8,128)(2,1)S(1)}, u32[]{:S(2)}, u32[]{:S(2)}) collective-permute-start(bf16[144,512]{1,0:T(8,128)(2,1)S(1)} %slice.8), channel_id=1, source_target_pairs={{0,24},{8,0},{16,8},{24,16},{1,25},{9,1},{17,9},{25,17},{2,26},{10... | collective-permute-start | bytes 442376 | tf_op jit(solution)/shard_map/ppermute | solution.py:288
  13.8 10.2 %collective-permute-start.3 = (bf16[144,512]{1,0:T(8,128)(2,1)S(1)}, bf16[144,512]{1,0:T(8,128)(2,1)S(1)}, u32[]{:S(2)}, u32[]{:S(2)}) collective-permute-start(bf16[144,512]{1,0:T(8,128)(2,1)S(1)} %slice.9), channel_id=1, source_target_pairs={{0,8},{8,16},{16,24},{24,0},{1,9},{9,17},{17,25},{25,1},{2,10},{10... | collective-permute-start | bytes 442376 | tf_op jit(solution)/shard_map/ppermute | solution.py:289
  20.7 9.9 %collective-permute-start.8 = (bf16[304,512]{1,0:T(8,128)(2,1)S(1)}, bf16[304,512]{1,0:T(8,128)(2,1)S(1)}, u32[]{:S(2)}, u32[]{:S(2)}) collective-permute-start(bf16[304,512]{1,0:T(8,128)(2,1)S(1)} %collective-permute-done.4.refs_0_), channel_id=1, source_target_pairs={{32,0},{64,32},{96,64},{128,96},{160,128},{192,160},{33,1},{65,33}... | collective-permute-start | bytes 933896 | tf_op jit(solution)/shard_map/ppermute | solution.py:294
  22.7 18.5 %collective-permute-start.9 = (bf16[304,512]{1,0:T(8,128)(2,1)S(1)}, bf16[304,512]{1,0:T(8,128)(2,1)S(1)}, u32[]{:S(2)}, u32[]{:S(2)}) collective-permute-start(bf16[304,512]{1,0:T(8,128)(2,1)S(1)} %collective-permute-done.5.refs_1_), channel_id=1, source_target_pairs={{192,224},{224,0},{0,32},{193,225},{225,1},{1,33},{194,226},{226,2... | collective-permute-start | bytes 933896 | tf_op jit(solution)/shard_map/ppermute | solution.py:296
  30.6 12.5 %collective-permute-start.12 = (bf16[304,512]{1,0:T(8,128)(2,1)S(1)}, bf16[304,512]{1,0:T(8,128)(2,1)S(1)}, u32[]{:S(2)}, u32[]{:S(2)}) collective-permute-start(bf16[304,512]{1,0:T(8,128)(2,1)S(1)} %collective-permute-done.8.refs_0_), channel_id=1, source_target_pairs={{32,0},{64,32},{96,64},{128,96},{160,128},{33,1},{65,33},{97,65},{... | collective-permute-start | bytes 933896 | tf_op jit(solution)/shard_map/ppermute | solution.py:294
  41.2 15.6 %collective-permute-start.14 = (bf16[304,512]{1,0:T(8,128)(2,1)S(1)}, bf16[304,512]{1,0:T(8,128)(2,1)S(1)}, u32[]{:S(2)}, u32[]{:S(2)}) collective-permute-start(bf16[304,512]{1,0:T(8,128)(2,1)S(1)} %collective-permute-done.9.refs_1_), channel_id=1, source_target_pairs={{224,0},{0,32},{32,64},{225,1},{1,33},{33,65},{226,2},{2,34},{34,6... | collective-permute-start | bytes 933896 | tf_op jit(solution)/shard_map/ppermute | solution.py:296
  43.2 13.7 %collective-permute-start.13 = (bf16[304,512]{1,0:T(8,128)(2,1)S(1)}, bf16[304,512]{1,0:T(8,128)(2,1)S(1)}, u32[]{:S(2)}, u32[]{:S(2)}) collective-permute-start(bf16[304,512]{1,0:T(8,128)(2,1)S(1)} %collective-permute-done.12.refs_0_), channel_id=1, source_target_pairs={{32,0},{64,32},{96,64},{128,96},{33,1},{65,33},{97,65},{129,97},{3... | collective-permute-start | bytes 933896 | tf_op jit(solution)/shard_map/ppermute | solution.py:294
  70.5 7.4 %collective-permute-start.23 = (bf16[288,256]{1,0:T(8,128)(2,1)S(1)}, bf16[288,256]{1,0:T(8,128)(2,1)S(1)}, u32[]{:S(2)}, u32[]{:S(2)}) collective-permute-start(bf16[288,256]{1,0:T(8,128)(2,1)S(1)} %get-tuple-element.49), channel_id=1, source_target_pairs={{0,24},{8,0},{16,8},{24,16},{1,25},{9,1},{17,9},{25,17},{2,26},{10... | collective-permute-start | bytes 442376 | tf_op jit(solution)/shard_map/ppermute | solution.py:320
  80.4 66.2 %all-to-all-start = ((bf16[32,64,256]{2,1,0:T(8,128)(2,1)}), bf16[32,64,256]{2,1,0:T(8,128)(2,1)S(1)}, u32[]{:S(2)}, u32[]{:S(2)}) async-start(bf16[32,64,256]{2,1,0:T(8,128)(2,1)} %bitcast.5), calls=%async_computation | async-start | bytes 2097152 | tf_op jit(solution)/shard_map/all_to_all | solution.py:337
  88.2 44.6 %collective-permute-start.24 = (bf16[4,288,256]{2,1,0:T(8,128)(2,1)S(1)}, bf16[4,288,256]{2,1,0:T(8,128)(2,1)S(1)}, u32[]{:S(2)}, u32[]{:S(2)}) collective-permute-start(bf16[4,288,256]{2,1,0:T(8,128)(2,1)S(1)} %get-tuple-element.52), channel_id=1, source_target_pairs={{0,1},{1,0},{2,3},{3,2},{4,5},{5,4},{6,7},{7,6},{8,9},{9,8},{10,11... | collective-permute-start | bytes 1769480 | tf_op jit(solution)/shard_map/ppermute | solution.py:353
  88.3 24.5 %collective-permute-start.6 = (bf16[288,256]{1,0:T(8,128)(2,1)S(1)}, bf16[288,256]{1,0:T(8,128)(2,1)S(1)}, u32[]{:S(2)}, u32[]{:S(2)}) collective-permute-start(bf16[288,256]{1,0:T(8,128)(2,1)S(1)} %copy-done.6), channel_id=1, source_target_pairs={{0,32},{32,64},{64,96},{96,128},{128,160},{160,192},{192,224},{1,3... | collective-permute-start | bytes 442376 | tf_op jit(solution)/shard_map/ppermute | solution.py:313
  91.7 24.1 %collective-permute-start.7 = (bf16[288,256]{1,0:T(8,128)(2,1)S(1)}, bf16[288,256]{1,0:T(8,128)(2,1)S(1)}, u32[]{:S(2)}, u32[]{:S(2)}) collective-permute-start(bf16[288,256]{1,0:T(8,128)(2,1)S(1)} %copy-done.4), channel_id=1, source_target_pairs={{0,224},{1,225},{2,226},{3,227},{4,228},{5,229},{6,230},{7,231},{8... | collective-permute-start | bytes 442376 | tf_op jit(solution)/shard_map/ppermute | solution.py:313
  92.4 24.3 %collective-permute-start.10 = (bf16[288,256]{1,0:T(8,128)(2,1)S(1)}, bf16[288,256]{1,0:T(8,128)(2,1)S(1)}, u32[]{:S(2)}, u32[]{:S(2)}) collective-permute-start(bf16[288,256]{1,0:T(8,128)(2,1)S(1)} %copy-done.8), channel_id=1, source_target_pairs={{0,64},{32,96},{64,128},{96,160},{128,192},{160,224},{1,65},{33,97... | collective-permute-start | bytes 442376 | tf_op jit(solution)/shard_map/ppermute | solution.py:313
  97.9 21.1 %collective-permute-start.16 = (bf16[288,256]{1,0:T(8,128)(2,1)S(1)}, bf16[288,256]{1,0:T(8,128)(2,1)S(1)}, u32[]{:S(2)}, u32[]{:S(2)}) collective-permute-start(bf16[288,256]{1,0:T(8,128)(2,1)S(1)} %copy-done.10), channel_id=1, source_target_pairs={{0,32},{32,64},{64,96},{96,128},{1,33},{33,65},{65,97},{97,129},{2... | collective-permute-start | bytes 442376 | tf_op jit(solution)/shard_map/ppermute | solution.py:317
  115.9 18.9 %collective-permute-start.18 = (bf16[288,256]{1,0:T(8,128)(2,1)S(1)}, bf16[288,256]{1,0:T(8,128)(2,1)S(1)}, u32[]{:S(2)}, u32[]{:S(2)}) collective-permute-start(bf16[288,256]{1,0:T(8,128)(2,1)S(1)} %get-tuple-element.43), channel_id=1, source_target_pairs={{0,8},{8,16},{16,24},{24,0},{1,9},{9,17},{17,25},{25,1},{2,10},{10... | collective-permute-start | bytes 442376 | tf_op jit(solution)/shard_map/ppermute | solution.py:321
  116.7 21.0 %collective-permute-start.19 = (bf16[288,256]{1,0:T(8,128)(2,1)S(1)}, bf16[288,256]{1,0:T(8,128)(2,1)S(1)}, u32[]{:S(2)}, u32[]{:S(2)}) collective-permute-start(bf16[288,256]{1,0:T(8,128)(2,1)S(1)} %get-tuple-element.44), channel_id=1, source_target_pairs={{0,16},{8,24},{16,0},{24,8},{1,17},{9,25},{17,1},{25,9},{2,18},{10... | collective-permute-start | bytes 442376 | tf_op jit(solution)/shard_map/ppermute | solution.py:321
  119.0 19.4 %collective-permute-start.20 = (bf16[288,256]{1,0:T(8,128)(2,1)S(1)}, bf16[288,256]{1,0:T(8,128)(2,1)S(1)}, u32[]{:S(2)}, u32[]{:S(2)}) collective-permute-start(bf16[288,256]{1,0:T(8,128)(2,1)S(1)} %get-tuple-element.45), channel_id=1, source_target_pairs={{0,24},{8,0},{16,8},{24,16},{1,25},{9,1},{17,9},{25,17},{2,26},{10... | collective-permute-start | bytes 442376 | tf_op jit(solution)/shard_map/ppermute | solution.py:321
  119.3 20.9 %collective-permute-start.15 = (bf16[288,256]{1,0:T(8,128)(2,1)S(1)}, bf16[288,256]{1,0:T(8,128)(2,1)S(1)}, u32[]{:S(2)}, u32[]{:S(2)}) collective-permute-start(bf16[288,256]{1,0:T(8,128)(2,1)S(1)} %get-tuple-element.39), channel_id=1, source_target_pairs={{0,160},{32,192},{64,224},{1,161},{33,193},{65,225},{2,162},{34,19... | collective-permute-start | bytes 442376 | tf_op jit(solution)/shard_map/ppermute | solution.py:313
  132.8 7.3 %collective-permute-start.17 = (bf16[288,256]{1,0:T(8,128)(2,1)S(1)}, bf16[288,256]{1,0:T(8,128)(2,1)S(1)}, u32[]{:S(2)}, u32[]{:S(2)}) collective-permute-start(bf16[288,256]{1,0:T(8,128)(2,1)S(1)} %added.3), channel_id=1, source_target_pairs={{0,96},{32,128},{64,160},{96,192},{128,224},{1,97},{33,129},{65,16... | collective-permute-start | bytes 442376 | tf_op jit(solution)/shard_map/ppermute | solution.py:319
  138.4 7.5 %collective-permute-start.25 = (bf16[288,256]{1,0:T(8,128)(2,1)S(1)}, bf16[288,256]{1,0:T(8,128)(2,1)S(1)}, u32[]{:S(2)}, u32[]{:S(2)}) collective-permute-start(bf16[288,256]{1,0:T(8,128)(2,1)S(1)} %get-tuple-element.54), channel_id=1, source_target_pairs={{0,2},{1,3},{2,4},{3,5},{4,6},{5,7},{6,0},{7,1},{8,10},{9,11},{10,... | collective-permute-start | bytes 442376 | tf_op jit(solution)/shard_map/ppermute | solution.py:366
  (21 other events, 144.8 us)

commit v3 on v2

--- a/solution.py
+++ b/solution.py
@@ -57,9 +57,22 @@
     out_ref[n : n + STAT_ROWS, 0:n] = jnp.where(is_low, stats - high, high).astype(BF16)
 
 
-def pack_keys_kernel(key_ref, latent_ref, weight_ref, out_ref):
-    out_ref[:, 0 : 2 * DV] = key_ref[...]
-    out_ref[:, 2 * DV :] = dot(latent_ref[...], weight_ref[...]).astype(BF16)
+def pack_keys_kernel(key_ref, latent_ref, weight_ref, out_ref, total_ref):
+    step = pl.program_id(0)
+    term = dot(latent_ref[...], weight_ref[...])
+
+    @pl.when(step == 0)
+    def _():
+        out_ref[:, 0 : 2 * DV] = key_ref[...]
+        total_ref[...] = term
+
+    @pl.when(step > 0)
+    def _():
+        total_ref[...] += term
+
+    @pl.when(step == pl.num_programs(0) - 1)
+    def _():
+        out_ref[:, 2 * DV :] = total_ref[...].astype(BF16)
 
 
 def attention_kernel(offsets, first_call, last_call, zy_ref, lam_ref, *refs):
@@ -276,9 +289,15 @@
     )(head_lambda, queries, out_first, out_second, cotangent, sums)
     keys_values = pl.pallas_call(
         pack_keys_kernel,
+        grid=(4,),
         out_shape=jax.ShapeDtypeStruct((n, 4 * DV), BF16),
-        in_specs=vmem(3),
-        out_specs=vmem(1)[0],
+        in_specs=[
+            pl.BlockSpec((n, 2 * DV), lambda i: (0, 0)),
+            pl.BlockSpec((n, latents.shape[1] // 4), lambda i: (0, i)),
+            pl.BlockSpec((latents.shape[1] // 4, 2 * DV), lambda i: (i, 0)),
+        ],
+        out_specs=pl.BlockSpec((n, 4 * DV), lambda i: (0, 0)),
+        scratch_shapes=[pltpu.VMEM((n, 2 * DV), F32)],
         cost_estimate=pl.CostEstimate(flops=10**9, bytes_accessed=3 * 10**6, transcendentals=0),
     )(key_vectors, latents, value_weight)
 

time: 148 us -> 149 us (level)
  no operation moved by 1% of the time
where the time goes in v3:
time: 149 us; the launch traced here: 148 us
  starting transfers between devices  70 us (47%)
  Pallas kernels  41.6 us (28%)
  waiting for transfers between devices  31.1 us (21%)
  local copies, waits for them, and re-layouts  3.13 us (2%)
  other arithmetic  1.57 us (1%)
    pallas_call x4, Pallas kernels, attention(): pl.pallas_call(functools.partial(attention_kernel, offsets, first_call, l...  29.4 us
    ppermute x5, starting transfers between devices, program(): lax.ppermute(term, 'z', [(i, i + d) for i in range(NZ - d)])  26.1 us
    ppermute x4, starting transfers between devices, program(): lax.ppermute(ahead[-1], 'z', [(k + 1, k) for k in range(NZ - t)])  14.3 us
    ppermute x5, waiting for transfers between devices, program(): lax.ppermute(term, 'z', [(i, i + d) for i in range(NZ - d)])  12.8 us
    ppermute x3, waiting for transfers between devices, program(): lax.ppermute(value_parts[e], 'y', ring(NY, e))  6.97 us
    all_to_all x1, starting transfers between devices, program(): lax.all_to_all(weight_term.reshape(NZ * NY, -1, 2 * DV), ('z', 'y'), spli...  5.7 us
    ppermute x4, waiting for transfers between devices, program(): lax.ppermute(ahead[-1], 'z', [(k + 1, k) for k in range(NZ - t)])  5.34 us
    ppermute x3, waiting for transfers between devices, program(): lax.ppermute(latent_parts[d], 'tp', ring(size, 2 * d)).astype(F32)  4.93 us
  transfers between devices with their start and end apart: 29, of which 11 were waited for; matrix products, arithmetic and copies ran while one was open for 1% of the time, Pallas kernels for 16%

profile of v3, /device:TPU:56, one launch (start us, length us, event | category | flops | bytes accessed | tf_op | source)
XLA Modules:
  0.0 148.5 jit_solution(5293190961483086407)
XLA Ops:
  0.6 3.8 %shard_map.121 = bf16[288,512]{1,0:T(8,128)(2,1)} custom-call(bf16[288,256]{1,0:T(8,128)(2,1)} %key_ref.1, bf16[288,2048]{1,0:T(8,128)(2,1)} %latent_ref.3, bf16[2048,256]{1,0:T(8,128)(2,1)} %weight_ref.3), custom_call_target="tpu_custom_call" | custom-call | flops 1000000000 | bytes 3000000 | tf_op jit(solution)/shard_map/pallas_call | solution.py:290
  5.2 2.5 %collective-permute-start.2 = (bf16[288,512]{1,0:T(8,128)(2,1)}, bf16[288,512]{1,0:T(8,128)(2,1)S(1)}, u32[]{:S(2)}, u32[]{:S(2)}) collective-permute-start(bf16[288,512]{1,0:T(8,128)(2,1)} %shard_map.121), channel_id=1, source_target_pairs={{0,8},{8,16},{16,24},{24,0},{1,9},{9,17},{17,25},{25,1},{2,10},{10... | collective-permute-start | bytes 884744 | tf_op jit(solution)/shard_map/ppermute | solution.py:306
  8.5 2.4 %shard_map.120.refs_0_ = bf16[304,512]{1,0:T(8,128)(2,1)} custom-call(f32[2]{0:T(128)} %lam_ref.9, bf16[288,256]{1,0:T(8,128)(2,1)} %q_ref.1, bf16[288,256]{1,0:T(8,128)(2,1)} %first_ref.1, bf16[288,256]{1,0:T(8,128)(2,1)} %second_ref.1, bf16[288,256]{1,0:T(8,128)(2,1)} %cot_ref.1, f32[16,288]{1,0:T(8,128)} %maximum_maximum_fusion.lse_ref), custom_call_target="tpu_custom_call" | custom-call | flops 1000000000 | bytes 1000000 | tf_op jit(solution)/shard_map/pallas_call | solution.py:283
  10.9 2.0 %collective-permute-start.4 = (bf16[304,512]{1,0:T(8,128)(2,1)}, bf16[304,512]{1,0:T(8,128)(2,1)S(1)}, u32[]{:S(2)}, u32[]{:S(2)}) collective-permute-start(bf16[304,512]{1,0:T(8,128)(2,1)} %shard_map.120.refs_0_), channel_id=1, source_target_pairs={{32,0},{64,32},{96,64},{128,96},{160,128},{192,160},{224,192},{33,... | collective-permute-start | bytes 933896 | tf_op jit(solution)/shard_map/ppermute | solution.py:313
  14.8 3.3 %collective-permute-start.3 = (bf16[144,512]{1,0:T(8,128)(2,1)S(1)}, bf16[144,512]{1,0:T(8,128)(2,1)S(1)}, u32[]{:S(2)}, u32[]{:S(2)}) collective-permute-start(bf16[144,512]{1,0:T(8,128)(2,1)S(1)} %slice.9), channel_id=1, source_target_pairs={{0,8},{8,16},{16,24},{24,0},{1,9},{9,17},{17,25},{25,1},{2,10},{10... | collective-permute-start | bytes 442376 | tf_op jit(solution)/shard_map/ppermute | solution.py:308
  18.1 3.6 %collective-permute-done.4.refs_0_ = bf16[304,512]{1,0:T(8,128)(2,1)S(1)} collective-permute-done((bf16[304,512]{1,0:T(8,128)(2,1)}, bf16[304,512]{1,0:T(8,128)(2,1)S(1)}, u32[]{:S(2)}, u32[]{:S(2)}) %collective-permute-start.4) | collective-permute-done | bytes 311328 | tf_op jit(solution)/shard_map/ppermute | solution.py:313
  25.1 4.7 %shard_map.122 = (f32[288,256]{1,0:T(8,128)S(1)}, f32[512,1152]{1,0:T(8,128)S(1)}) custom-call(s32[2]{0:T(128)S(1)} %pad_add_fusion.zy_ref, f32[2]{0:T(128)S(1)} %copy-done.11, bf16[304,512]{1,0:T(8,128)(2,1)S(1)} %copy-done.2, bf16[1152,512]{1,0:T(8,128)(2,1)S(1)} %constant_dynamic-update-slice_fusion.refs_1_.refs_2_.refs_3_), custom_call_target="tpu_custom_call" | custom-call | flops 4000000000 | bytes 1000000 | tf_op jit(solution)/shard_map/pallas_call | solution.py:240
  31.6 5.5 %collective-permute-start.12 = (bf16[304,512]{1,0:T(8,128)(2,1)S(1)}, bf16[304,512]{1,0:T(8,128)(2,1)S(1)}, u32[]{:S(2)}, u32[]{:S(2)}) collective-permute-start(bf16[304,512]{1,0:T(8,128)(2,1)S(1)} %collective-permute-done.8.refs_0_), channel_id=1, source_target_pairs={{32,0},{64,32},{96,64},{128,96},{160,128},{33,1},{65,33},{97,65},{... | collective-permute-start | bytes 933896 | tf_op jit(solution)/shard_map/ppermute | solution.py:313
  37.1 4.5 %shard_map.123 = (bf16[288,256]{1,0:T(8,128)(2,1)S(1)}, bf16[288,256]{1,0:T(8,128)(2,1)S(1)}, f32[512,1152]{1,0:T(8,128)S(1)}) custom-call(s32[2]{0:T(128)S(1)} %pad_add_fusion.zy_ref, f32[2]{0:T(128)S(1)} %copy-done.11, bf16[304,512]{1,0:T(8,128)(2,1)S(1)} %collective-permute-done.4.refs_0_, bf16[304,512]{1,0:T(8,128)(2,1)S(1)} %collective-permute-done.5.refs_1_, ...), custom_call_target="tpu_custom_call" | custom-call | flops 8000000000 | bytes 2000000 | tf_op jit(solution)/shard_map/pallas_call | solution.py:240
  44.2 4.8 %collective-permute-start.13 = (bf16[304,512]{1,0:T(8,128)(2,1)S(1)}, bf16[304,512]{1,0:T(8,128)(2,1)S(1)}, u32[]{:S(2)}, u32[]{:S(2)}) collective-permute-start(bf16[304,512]{1,0:T(8,128)(2,1)S(1)} %collective-permute-done.12.refs_0_), channel_id=1, source_target_pairs={{32,0},{64,32},{96,64},{128,96},{33,1},{65,33},{97,65},{129,97},{3... | collective-permute-start | bytes 933896 | tf_op jit(solution)/shard_map/ppermute | solution.py:313
  49.0 8.2 %shard_map.124 = (bf16[288,256]{1,0:T(8,128)(2,1)S(1)}, bf16[288,256]{1,0:T(8,128)(2,1)S(1)}, f32[512,1152]{1,0:T(8,128)S(1)}) custom-call(s32[2]{0:T(128)S(1)} %pad_add_fusion.zy_ref, f32[2]{0:T(128)S(1)} %copy-done.11, bf16[304,512]{1,0:T(8,128)(2,1)S(1)} %collective-permute-done.8.refs_0_, bf16[304,512]{1,0:T(8,128)(2,1)S(1)} %collective-permute-done.9.refs_1_, ...), custom_call_target="tpu_custom_call" | custom-call | flops 8000000000 | bytes 2000000 | tf_op jit(solution)/shard_map/pallas_call | solution.py:240
  57.9 12.0 %shard_map.125 = (bf16[288,256]{1,0:T(8,128)(2,1)S(1)}, bf16[288,256]{1,0:T(8,128)(2,1)S(1)}, bf16[288,256]{1,0:T(8,128)(2,1)S(1)}, bf16[288,256]{1,0:T(8,128)(2...) custom-call(s32[2]{0:T(128)S(1)} %pad_add_fusion.zy_ref, ...), custom_call_target="tpu_custom_call" | custom-call | flops 12000000000 | bytes 3000000 | tf_op jit(solution)/shard_map/pallas_call | solution.py:240
  72.0 3.4 %collective-permute-done.21.refs_1_ = bf16[288,256]{1,0:T(8,128)(2,1)S(1)} collective-permute-done((bf16[288,256]{1,0:T(8,128)(2,1)S(1)}, bf16[288,256]{1,0:T(8,128)(2,1)S(1)}, u32[]{:S(2)}, u32[]{:S(2)}) %collective-permute-start.21) | collective-permute-done | bytes 147488 | tf_op jit(solution)/shard_map/ppermute | solution.py:339
  75.4 2.1 %collective-permute-done.22.refs_2_ = bf16[288,256]{1,0:T(8,128)(2,1)S(1)} collective-permute-done((bf16[288,256]{1,0:T(8,128)(2,1)S(1)}, bf16[288,256]{1,0:T(8,128)(2,1)S(1)}, u32[]{:S(2)}, u32[]{:S(2)}) %collective-permute-start.22) | collective-permute-done | bytes 147488 | tf_op jit(solution)/shard_map/ppermute | solution.py:339
  81.5 5.7 %all-to-all-start = ((bf16[32,64,256]{2,1,0:T(8,128)(2,1)}), bf16[32,64,256]{2,1,0:T(8,128)(2,1)S(1)}, u32[]{:S(2)}, u32[]{:S(2)}) async-start(bf16[32,64,256]{2,1,0:T(8,128)(2,1)} %bitcast.5), calls=%async_computation | async-start | bytes 2097152 | tf_op jit(solution)/shard_map/all_to_all | solution.py:356
  89.3 3.4 %collective-permute-start.6 = (bf16[288,256]{1,0:T(8,128)(2,1)S(1)}, bf16[288,256]{1,0:T(8,128)(2,1)S(1)}, u32[]{:S(2)}, u32[]{:S(2)}) collective-permute-start(bf16[288,256]{1,0:T(8,128)(2,1)S(1)} %copy-done.6), channel_id=1, source_target_pairs={{0,32},{32,64},{64,96},{96,128},{128,160},{160,192},{192,224},{1,3... | collective-permute-start | bytes 442376 | tf_op jit(solution)/shard_map/ppermute | solution.py:332
  93.4 5.5 %collective-permute-start.10 = (bf16[288,256]{1,0:T(8,128)(2,1)S(1)}, bf16[288,256]{1,0:T(8,128)(2,1)S(1)}, u32[]{:S(2)}, u32[]{:S(2)}) collective-permute-start(bf16[288,256]{1,0:T(8,128)(2,1)S(1)} %copy-done.8), channel_id=1, source_target_pairs={{0,64},{32,96},{64,128},{96,160},{128,192},{160,224},{1,65},{33,97... | collective-permute-start | bytes 442376 | tf_op jit(solution)/shard_map/ppermute | solution.py:332
  98.9 2.5 %collective-permute-start.16 = (bf16[288,256]{1,0:T(8,128)(2,1)S(1)}, bf16[288,256]{1,0:T(8,128)(2,1)S(1)}, u32[]{:S(2)}, u32[]{:S(2)}) collective-permute-start(bf16[288,256]{1,0:T(8,128)(2,1)S(1)} %copy-done.10), channel_id=1, source_target_pairs={{0,32},{32,64},{64,96},{96,128},{1,33},{33,65},{65,97},{97,129},{2... | collective-permute-start | bytes 442376 | tf_op jit(solution)/shard_map/ppermute | solution.py:336
  101.4 12.4 %collective-permute-done.6.refs_1_ = bf16[288,256]{1,0:T(8,128)(2,1)S(1)} collective-permute-done((bf16[288,256]{1,0:T(8,128)(2,1)S(1)}, bf16[288,256]{1,0:T(8,128)(2,1)S(1)}, u32[]{:S(2)}, u32[]{:S(2)}) %collective-permute-start.6) | collective-permute-done | bytes 147488 | tf_op jit(solution)/shard_map/ppermute | solution.py:332
  113.8 3.1 %collective-permute-start.11 = (bf16[288,256]{1,0:T(8,128)(2,1)S(1)}, bf16[288,256]{1,0:T(8,128)(2,1)S(1)}, u32[]{:S(2)}, u32[]{:S(2)}) collective-permute-start(bf16[288,256]{1,0:T(8,128)(2,1)S(1)} %get-tuple-element.37), channel_id=1, source_target_pairs={{0,192},{32,224},{1,193},{33,225},{2,194},{34,226},{3,195},{35,227... | collective-permute-start | bytes 442376 | tf_op jit(solution)/shard_map/ppermute | solution.py:332
  117.7 2.3 %collective-permute-start.19 = (bf16[288,256]{1,0:T(8,128)(2,1)S(1)}, bf16[288,256]{1,0:T(8,128)(2,1)S(1)}, u32[]{:S(2)}, u32[]{:S(2)}) collective-permute-start(bf16[288,256]{1,0:T(8,128)(2,1)S(1)} %get-tuple-element.44), channel_id=1, source_target_pairs={{0,16},{8,24},{16,0},{24,8},{1,17},{9,25},{17,1},{25,9},{2,18},{10... | collective-permute-start | bytes 442376 | tf_op jit(solution)/shard_map/ppermute | solution.py:340
  120.3 13.5 %collective-permute-start.15 = (bf16[288,256]{1,0:T(8,128)(2,1)S(1)}, bf16[288,256]{1,0:T(8,128)(2,1)S(1)}, u32[]{:S(2)}, u32[]{:S(2)}) collective-permute-start(bf16[288,256]{1,0:T(8,128)(2,1)S(1)} %get-tuple-element.39), channel_id=1, source_target_pairs={{0,160},{32,192},{64,224},{1,161},{33,193},{65,225},{2,162},{34,19... | collective-permute-start | bytes 442376 | tf_op jit(solution)/shard_map/ppermute | solution.py:332
  135.8 2.9 %collective-permute-start.27 = (bf16[288,256]{1,0:T(8,128)(2,1)S(1)}, bf16[288,256]{1,0:T(8,128)(2,1)S(1)}, u32[]{:S(2)}, u32[]{:S(2)}) collective-permute-start(bf16[288,256]{1,0:T(8,128)(2,1)S(1)} %get-tuple-element.56), channel_id=1, source_target_pairs={{0,6},{1,7},{2,0},{3,1},{4,2},{5,3},{6,4},{7,5},{8,14},{9,15},{10,... | collective-permute-start | bytes 442376 | tf_op jit(solution)/shard_map/ppermute | solution.py:385
  143.0 2.5 %collective-permute-done.26 = bf16[288,256]{1,0:T(8,128)(2,1)S(1)} collective-permute-done((bf16[288,256]{1,0:T(8,128)(2,1)S(1)}, bf16[288,256]{1,0:T(8,128)(2,1)S(1)}, u32[]{:S(2)}, u32[]{:S(2)}) %collective-permute-start.26) | collective-permute-done | bytes 147488 | tf_op jit(solution)/shard_map/ppermute | solution.py:385
  (92 shorter events, 30.9 us)
Async XLA Ops:
  4.5 10.2 %collective-permute-start = (bf16[288,512]{1,0:T(8,128)(2,1)}, bf16[288,512]{1,0:T(8,128)(2,1)S(1)}, u32[]{:S(2)}, u32[]{:S(2)}) collective-permute-start(bf16[288,512]{1,0:T(8,128)(2,1)} %shard_map.121), channel_id=1, source_target_pairs={{0,24},{8,0},{16,8},{24,16},{1,25},{9,1},{17,9},{25,17},{2,26},{10... | collective-permute-start | bytes 884744 | tf_op jit(solution)/shard_map/ppermute | solution.py:305
  5.2 9.6 %collective-permute-start.2 = (bf16[288,512]{1,0:T(8,128)(2,1)}, bf16[288,512]{1,0:T(8,128)(2,1)S(1)}, u32[]{:S(2)}, u32[]{:S(2)}) collective-permute-start(bf16[288,512]{1,0:T(8,128)(2,1)} %shard_map.121), channel_id=1, source_target_pairs={{0,8},{8,16},{16,24},{24,0},{1,9},{9,17},{17,25},{25,1},{2,10},{10... | collective-permute-start | bytes 884744 | tf_op jit(solution)/shard_map/ppermute | solution.py:306
  10.9 10.8 %collective-permute-start.4 = (bf16[304,512]{1,0:T(8,128)(2,1)}, bf16[304,512]{1,0:T(8,128)(2,1)S(1)}, u32[]{:S(2)}, u32[]{:S(2)}) collective-permute-start(bf16[304,512]{1,0:T(8,128)(2,1)} %shard_map.120.refs_0_), channel_id=1, source_target_pairs={{32,0},{64,32},{96,64},{128,96},{160,128},{192,160},{224,192},{33,... | collective-permute-start | bytes 933896 | tf_op jit(solution)/shard_map/ppermute | solution.py:313
  12.9 10.8 %collective-permute-start.5 = (bf16[304,512]{1,0:T(8,128)(2,1)}, bf16[304,512]{1,0:T(8,128)(2,1)S(1)}, u32[]{:S(2)}, u32[]{:S(2)}) collective-permute-start(bf16[304,512]{1,0:T(8,128)(2,1)} %shard_map.120.refs_0_), channel_id=1, source_target_pairs={{160,192},{192,224},{224,0},{161,193},{193,225},{225,1},{162,194},... | collective-permute-start | bytes 933896 | tf_op jit(solution)/shard_map/ppermute | solution.py:315
  14.6 10.4 %collective-permute-start.1 = (bf16[144,512]{1,0:T(8,128)(2,1)S(1)}, bf16[144,512]{1,0:T(8,128)(2,1)S(1)}, u32[]{:S(2)}, u32[]{:S(2)}) collective-permute-start(bf16[144,512]{1,0:T(8,128)(2,1)S(1)} %slice.8), channel_id=1, source_target_pairs={{0,24},{8,0},{16,8},{24,16},{1,25},{9,1},{17,9},{25,17},{2,26},{10... | collective-permute-start | bytes 442376 | tf_op jit(solution)/shard_map/ppermute | solution.py:307
  14.8 10.2 %collective-permute-start.3 = (bf16[144,512]{1,0:T(8,128)(2,1)S(1)}, bf16[144,512]{1,0:T(8,128)(2,1)S(1)}, u32[]{:S(2)}, u32[]{:S(2)}) collective-permute-start(bf16[144,512]{1,0:T(8,128)(2,1)S(1)} %slice.9), channel_id=1, source_target_pairs={{0,8},{8,16},{16,24},{24,0},{1,9},{9,17},{17,25},{25,1},{2,10},{10... | collective-permute-start | bytes 442376 | tf_op jit(solution)/shard_map/ppermute | solution.py:308
  21.7 9.9 %collective-permute-start.8 = (bf16[304,512]{1,0:T(8,128)(2,1)S(1)}, bf16[304,512]{1,0:T(8,128)(2,1)S(1)}, u32[]{:S(2)}, u32[]{:S(2)}) collective-permute-start(bf16[304,512]{1,0:T(8,128)(2,1)S(1)} %collective-permute-done.4.refs_0_), channel_id=1, source_target_pairs={{32,0},{64,32},{96,64},{128,96},{160,128},{192,160},{33,1},{65,33}... | collective-permute-start | bytes 933896 | tf_op jit(solution)/shard_map/ppermute | solution.py:313
  23.7 18.5 %collective-permute-start.9 = (bf16[304,512]{1,0:T(8,128)(2,1)S(1)}, bf16[304,512]{1,0:T(8,128)(2,1)S(1)}, u32[]{:S(2)}, u32[]{:S(2)}) collective-permute-start(bf16[304,512]{1,0:T(8,128)(2,1)S(1)} %collective-permute-done.5.refs_1_), channel_id=1, source_target_pairs={{192,224},{224,0},{0,32},{193,225},{225,1},{1,33},{194,226},{226,2... | collective-permute-start | bytes 933896 | tf_op jit(solution)/shard_map/ppermute | solution.py:315
  31.6 12.5 %collective-permute-start.12 = (bf16[304,512]{1,0:T(8,128)(2,1)S(1)}, bf16[304,512]{1,0:T(8,128)(2,1)S(1)}, u32[]{:S(2)}, u32[]{:S(2)}) collective-permute-start(bf16[304,512]{1,0:T(8,128)(2,1)S(1)} %collective-permute-done.8.refs_0_), channel_id=1, source_target_pairs={{32,0},{64,32},{96,64},{128,96},{160,128},{33,1},{65,33},{97,65},{... | collective-permute-start | bytes 933896 | tf_op jit(solution)/shard_map/ppermute | solution.py:313
  42.2 15.6 %collective-permute-start.14 = (bf16[304,512]{1,0:T(8,128)(2,1)S(1)}, bf16[304,512]{1,0:T(8,128)(2,1)S(1)}, u32[]{:S(2)}, u32[]{:S(2)}) collective-permute-start(bf16[304,512]{1,0:T(8,128)(2,1)S(1)} %collective-permute-done.9.refs_1_), channel_id=1, source_target_pairs={{224,0},{0,32},{32,64},{225,1},{1,33},{33,65},{226,2},{2,34},{34,6... | collective-permute-start | bytes 933896 | tf_op jit(solution)/shard_map/ppermute | solution.py:315
  44.2 13.7 %collective-permute-start.13 = (bf16[304,512]{1,0:T(8,128)(2,1)S(1)}, bf16[304,512]{1,0:T(8,128)(2,1)S(1)}, u32[]{:S(2)}, u32[]{:S(2)}) collective-permute-start(bf16[304,512]{1,0:T(8,128)(2,1)S(1)} %collective-permute-done.12.refs_0_), channel_id=1, source_target_pairs={{32,0},{64,32},{96,64},{128,96},{33,1},{65,33},{97,65},{129,97},{3... | collective-permute-start | bytes 933896 | tf_op jit(solution)/shard_map/ppermute | solution.py:313
  71.6 7.4 %collective-permute-start.23 = (bf16[288,256]{1,0:T(8,128)(2,1)S(1)}, bf16[288,256]{1,0:T(8,128)(2,1)S(1)}, u32[]{:S(2)}, u32[]{:S(2)}) collective-permute-start(bf16[288,256]{1,0:T(8,128)(2,1)S(1)} %get-tuple-element.49), channel_id=1, source_target_pairs={{0,24},{8,0},{16,8},{24,16},{1,25},{9,1},{17,9},{25,17},{2,26},{10... | collective-permute-start | bytes 442376 | tf_op jit(solution)/shard_map/ppermute | solution.py:339
  81.5 66.2 %all-to-all-start = ((bf16[32,64,256]{2,1,0:T(8,128)(2,1)}), bf16[32,64,256]{2,1,0:T(8,128)(2,1)S(1)}, u32[]{:S(2)}, u32[]{:S(2)}) async-start(bf16[32,64,256]{2,1,0:T(8,128)(2,1)} %bitcast.5), calls=%async_computation | async-start | bytes 2097152 | tf_op jit(solution)/shard_map/all_to_all | solution.py:356
  89.2 44.6 %collective-permute-start.24 = (bf16[4,288,256]{2,1,0:T(8,128)(2,1)S(1)}, bf16[4,288,256]{2,1,0:T(8,128)(2,1)S(1)}, u32[]{:S(2)}, u32[]{:S(2)}) collective-permute-start(bf16[4,288,256]{2,1,0:T(8,128)(2,1)S(1)} %get-tuple-element.52), channel_id=1, source_target_pairs={{0,1},{1,0},{2,3},{3,2},{4,5},{5,4},{6,7},{7,6},{8,9},{9,8},{10,11... | collective-permute-start | bytes 1769480 | tf_op jit(solution)/shard_map/ppermute | solution.py:372
  89.3 24.5 %collective-permute-start.6 = (bf16[288,256]{1,0:T(8,128)(2,1)S(1)}, bf16[288,256]{1,0:T(8,128)(2,1)S(1)}, u32[]{:S(2)}, u32[]{:S(2)}) collective-permute-start(bf16[288,256]{1,0:T(8,128)(2,1)S(1)} %copy-done.6), channel_id=1, source_target_pairs={{0,32},{32,64},{64,96},{96,128},{128,160},{160,192},{192,224},{1,3... | collective-permute-start | bytes 442376 | tf_op jit(solution)/shard_map/ppermute | solution.py:332
  92.7 24.2 %collective-permute-start.7 = (bf16[288,256]{1,0:T(8,128)(2,1)S(1)}, bf16[288,256]{1,0:T(8,128)(2,1)S(1)}, u32[]{:S(2)}, u32[]{:S(2)}) collective-permute-start(bf16[288,256]{1,0:T(8,128)(2,1)S(1)} %copy-done.4), channel_id=1, source_target_pairs={{0,224},{1,225},{2,226},{3,227},{4,228},{5,229},{6,230},{7,231},{8... | collective-permute-start | bytes 442376 | tf_op jit(solution)/shard_map/ppermute | solution.py:332
  93.4 24.3 %collective-permute-start.10 = (bf16[288,256]{1,0:T(8,128)(2,1)S(1)}, bf16[288,256]{1,0:T(8,128)(2,1)S(1)}, u32[]{:S(2)}, u32[]{:S(2)}) collective-permute-start(bf16[288,256]{1,0:T(8,128)(2,1)S(1)} %copy-done.8), channel_id=1, source_target_pairs={{0,64},{32,96},{64,128},{96,160},{128,192},{160,224},{1,65},{33,97... | collective-permute-start | bytes 442376 | tf_op jit(solution)/shard_map/ppermute | solution.py:332
  98.9 21.1 %collective-permute-start.16 = (bf16[288,256]{1,0:T(8,128)(2,1)S(1)}, bf16[288,256]{1,0:T(8,128)(2,1)S(1)}, u32[]{:S(2)}, u32[]{:S(2)}) collective-permute-start(bf16[288,256]{1,0:T(8,128)(2,1)S(1)} %copy-done.10), channel_id=1, source_target_pairs={{0,32},{32,64},{64,96},{96,128},{1,33},{33,65},{65,97},{97,129},{2... | collective-permute-start | bytes 442376 | tf_op jit(solution)/shard_map/ppermute | solution.py:336
  116.9 18.9 %collective-permute-start.18 = (bf16[288,256]{1,0:T(8,128)(2,1)S(1)}, bf16[288,256]{1,0:T(8,128)(2,1)S(1)}, u32[]{:S(2)}, u32[]{:S(2)}) collective-permute-start(bf16[288,256]{1,0:T(8,128)(2,1)S(1)} %get-tuple-element.43), channel_id=1, source_target_pairs={{0,8},{8,16},{16,24},{24,0},{1,9},{9,17},{17,25},{25,1},{2,10},{10... | collective-permute-start | bytes 442376 | tf_op jit(solution)/shard_map/ppermute | solution.py:340
  117.7 21.0 %collective-permute-start.19 = (bf16[288,256]{1,0:T(8,128)(2,1)S(1)}, bf16[288,256]{1,0:T(8,128)(2,1)S(1)}, u32[]{:S(2)}, u32[]{:S(2)}) collective-permute-start(bf16[288,256]{1,0:T(8,128)(2,1)S(1)} %get-tuple-element.44), channel_id=1, source_target_pairs={{0,16},{8,24},{16,0},{24,8},{1,17},{9,25},{17,1},{25,9},{2,18},{10... | collective-permute-start | bytes 442376 | tf_op jit(solution)/shard_map/ppermute | solution.py:340
  120.0 19.5 %collective-permute-start.20 = (bf16[288,256]{1,0:T(8,128)(2,1)S(1)}, bf16[288,256]{1,0:T(8,128)(2,1)S(1)}, u32[]{:S(2)}, u32[]{:S(2)}) collective-permute-start(bf16[288,256]{1,0:T(8,128)(2,1)S(1)} %get-tuple-element.45), channel_id=1, source_target_pairs={{0,24},{8,0},{16,8},{24,16},{1,25},{9,1},{17,9},{25,17},{2,26},{10... | collective-permute-start | bytes 442376 | tf_op jit(solution)/shard_map/ppermute | solution.py:340
  120.3 20.8 %collective-permute-start.15 = (bf16[288,256]{1,0:T(8,128)(2,1)S(1)}, bf16[288,256]{1,0:T(8,128)(2,1)S(1)}, u32[]{:S(2)}, u32[]{:S(2)}) collective-permute-start(bf16[288,256]{1,0:T(8,128)(2,1)S(1)} %get-tuple-element.39), channel_id=1, source_target_pairs={{0,160},{32,192},{64,224},{1,161},{33,193},{65,225},{2,162},{34,19... | collective-permute-start | bytes 442376 | tf_op jit(solution)/shard_map/ppermute | solution.py:332
  133.8 7.3 %collective-permute-start.17 = (bf16[288,256]{1,0:T(8,128)(2,1)S(1)}, bf16[288,256]{1,0:T(8,128)(2,1)S(1)}, u32[]{:S(2)}, u32[]{:S(2)}) collective-permute-start(bf16[288,256]{1,0:T(8,128)(2,1)S(1)} %added.3), channel_id=1, source_target_pairs={{0,96},{32,128},{64,160},{96,192},{128,224},{1,97},{33,129},{65,16... | collective-permute-start | bytes 442376 | tf_op jit(solution)/shard_map/ppermute | solution.py:338
  139.5 7.5 %collective-permute-start.25 = (bf16[288,256]{1,0:T(8,128)(2,1)S(1)}, bf16[288,256]{1,0:T(8,128)(2,1)S(1)}, u32[]{:S(2)}, u32[]{:S(2)}) collective-permute-start(bf16[288,256]{1,0:T(8,128)(2,1)S(1)} %get-tuple-element.54), channel_id=1, source_target_pairs={{0,2},{1,3},{2,4},{3,5},{4,6},{5,7},{6,0},{7,1},{8,10},{9,11},{10,... | collective-permute-start | bytes 442376 | tf_op jit(solution)/shard_map/ppermute | solution.py:385
  (21 other events, 145.8 us)
